TPU v7x, 32 devices: a whole 2x2x4 slice. The times are simulated.
32 devices in a mesh: fs: 8 (over z, x), tp: 4 (over y, core).
Axes of the slice: x: 2, y: 2, z: 4, core: 2. Of those that a mesh axis runs over, the one named last changes fastest.
Arguments:
- tokens: bfloat16 [3072, 4096], P('fs', 'tp'), may hold values from -600 to 600
- gate_master: float32 [8, 4096, 512], P(None, 'fs', 'tp'), may hold values from -0.09375 to 0.09375
- up_master: float32 [8, 4096, 512], P(None, 'fs', 'tp'), may hold values from -0.09375 to 0.09375
- down_master: float32 [8, 4096, 512], P(None, 'fs', 'tp'), may hold values from -0.25 to 0.25
- norm_gain: float32 [4096], P('fs'), may hold values from 0.1 to 1.9
- routes: int32 [3072, 2], P('fs'), may hold values from 0 to 7, all different within a row; in each aligned block of 384 rows (0 to 383, 384 to 767, ...) at most 192 rows name the same one
- route_weight: float32 [3072, 2], P('fs'), may hold values from 0.1 to 1
Outputs:
- gate_out: bfloat16 [8, 4096, 512], P('fs', None, 'tp')
- up_out: bfloat16 [8, 4096, 512], P('fs', None, 'tp')
- down_out: bfloat16 [8, 4096, 512], P('fs', None, 'tp')
- mixed: bfloat16 [3072, 4096], P('fs', 'tp')
Inputs may be any that keep to these rules, and one draw needn't show every extreme that they name: `routes`: within the rows of one index of fs no expert is named by more than 192 pairs, a bound that some block reaches; the 2 experts of a row differ.
All inputs are finite; a program needn't handle non-finite values.
Results may differ from a plain program's by a relative error of at most 0.0087.
Values may be sent and summed in bfloat16 or wider, within the bound.
A program may use at most 128 MiB of HBM per device.

v0:
```python
import jax
import jax.numpy as jnp
from jax import lax
from jax.sharding import PartitionSpec as P

norm_eps = 1e-06


def half_shift(step, size):
    half = size // 2
    return [(s, s // half * half + (s % half + step) % half) for s in range(size)]


def cross_swap(size):
    return [(s, (s + size // 2) % size) for s in range(size)]


def member_shift(step, crossed, size):
    half = size // 2
    return [
        (s, (s // half + crossed) % 2 * half + (s % half + step) % half) for s in range(size)
    ]


def body(tokens, gate_master, up_master, down_master, norm_gain, routes, route_weight):
    n_experts = gate_master.shape[0]
    tok_rows, top_count = routes.shape
    capacity = 2 * tok_rows * top_count // n_experts
    n_tp = lax.axis_size("tp")
    half = n_tp // 2
    width = tokens.shape[1]
    hidden_cols = gate_master.shape[2]
    me_tp = lax.axis_index("tp")
    chunks = 2 if capacity % 32 == 0 else 1
    part = capacity // chunks

    folded = norm_gain[None, :, None]
    trio = jnp.concatenate(
        [
            (gate_master * folded).astype(jnp.bfloat16),
            (up_master * folded).astype(jnp.bfloat16),
            down_master.astype(jnp.bfloat16),
        ],
        axis=2,
    )
    trio = lax.all_to_all(trio, "fs", split_axis=0, concat_axis=1, tiled=True)
    pair = trio[:, :, : 2 * hidden_cols]
    gate_out = trio[:, :, :hidden_cols]
    up_out = trio[:, :, hidden_cols : 2 * hidden_cols]
    down_out = trio[:, :, 2 * hidden_cols :]

    token_float = tokens.astype(jnp.float32)
    sumsquares = lax.psum(jnp.sum(token_float * token_float, axis=1), "tp")
    inverse = lax.rsqrt(sumsquares / (width * n_tp) + norm_eps)[:, None]
    normed = (token_float * inverse).astype(jnp.bfloat16)
    mix = route_weight / jnp.sum(route_weight, axis=1, keepdims=True)
    experts = jnp.arange(n_experts, dtype=jnp.int32)
    named = jnp.any(routes[:, :, None] == experts, axis=1)
    earlier = jnp.arange(tok_rows)[:, None] > jnp.arange(tok_rows)[None, :]
    before = jnp.dot(
        earlier.astype(jnp.bfloat16), named.astype(jnp.bfloat16), preferred_element_type=jnp.float32
    ).astype(jnp.int32)
    slots = jnp.sum(jnp.where(routes[:, :, None] == experts, before[:, None, :], 0), axis=2)
    place = (slots // part * n_experts + routes) * part + slots % part
    spots = jnp.arange(n_experts * capacity, dtype=jnp.int32)
    where_to = place[:, :, None] == spots
    onehot = jnp.any(where_to, axis=1).astype(jnp.bfloat16)
    mixing = jnp.sum(jnp.where(where_to, mix[:, :, None], 0.0), axis=1)
    mixing = mixing.astype(jnp.bfloat16)
    outgoing = lax.dot_general(
        onehot, normed, (((0,), (0,)), ((), ())), preferred_element_type=jnp.float32
    ).astype(jnp.bfloat16)
    outgoing = outgoing.reshape(chunks, n_experts, part, width)

    my_half = me_tp // half
    inside = me_tp % half
    span = half * width
    own_cols = lax.dynamic_slice_in_dim(pair[0], my_half * span, span, 0)
    partner_cols = lax.ppermute(
        lax.dynamic_slice_in_dim(pair[0], (1 - my_half) * span, span, 0), "tp", cross_swap(n_tp)
    )

    arrived = []
    for c in range(chunks):
        if c == 0:
            ready, trio = lax.optimization_barrier((outgoing[c], trio))
        else:
            ready, arrived[-1], partner_cols = lax.optimization_barrier((outgoing[c], last, partner_cols))
        last = lax.all_to_all(ready, "fs", split_axis=0, concat_axis=0, tiled=True)
        arrived.append(last)

    def in_order(cols):
        blocks = cols.reshape(half, width, cols.shape[1])
        return [
            lax.dynamic_index_in_dim(blocks, (inside + half - j) % half, 0, keepdims=False)
            for j in range(half)
        ]

    own_blocks, partner_blocks = in_order(own_cols), in_order(partner_cols)
    quarters = down_out[0].reshape(n_tp, -1, hidden_cols)
    picked = []
    for j in range(half):
        for crossed in range(2):
            target = (my_half + crossed) % 2 * half + (inside + j) % half
            piece = lax.dynamic_index_in_dim(quarters, target, 0, keepdims=False)
            if j + crossed > 0:
                piece = lax.ppermute(piece, "tp", member_shift(j, crossed, n_tp))
            picked.append(piece)
    down_mat = jnp.concatenate(picked, axis=1)

    def serve(rows):
        rows = rows.reshape(-1, width)
        pieces = [rows] + [lax.ppermute(rows, "tp", half_shift(j, n_tp)) for j in range(1, half)]

        def partial(blocks):
            total = 0.0
            for piece, block in zip(pieces, blocks):
                total = total + jnp.dot(piece, block, preferred_element_type=jnp.float32)
            return total

        swapped = lax.ppermute(partial(partner_blocks).astype(jnp.bfloat16), "tp", cross_swap(n_tp))
        both = partial(own_blocks) + swapped.astype(jnp.float32)
        hidden = (jax.nn.silu(both[:, :hidden_cols]) * both[:, hidden_cols:]).astype(jnp.bfloat16)
        two = jnp.concatenate([hidden, lax.ppermute(hidden, "tp", cross_swap(n_tp))], axis=1)
        all_hidden = [two] + [lax.ppermute(two, "tp", half_shift(j, n_tp)) for j in range(1, half)]
        result = lax.dot_general(
            jnp.concatenate(all_hidden, axis=1),
            down_mat,
            (((1,), (1,)), ((), ())),
            preferred_element_type=jnp.float32,
        )
        return result.astype(jnp.bfloat16).reshape(-1, part, width)

    returned = []
    for c in range(chunks):
        rows = arrived[c]
        if c > 0:
            rows, served = lax.optimization_barrier((rows, served))
            returned.append(lax.all_to_all(served, "fs", split_axis=0, concat_axis=0, tiled=True))
        served = serve(rows)
    returned.append(lax.all_to_all(served, "fs", split_axis=0, concat_axis=0, tiled=True))

    mixed = 0.0
    for c, back in enumerate(returned):
        flat = back.reshape(n_experts * part, width)
        chosen = mixing[:, c * n_experts * part : (c + 1) * n_experts * part]
        mixed = mixed + jnp.dot(chosen, flat, preferred_element_type=jnp.float32)
    return (gate_out, up_out, down_out, mixed.astype(jnp.bfloat16))


def solution(mesh):
    placed = (
        P("fs", "tp"),
        P(None, "fs", "tp"),
        P(None, "fs", "tp"),
        P(None, "fs", "tp"),
        P("fs"),
        P("fs", None),
        P("fs", None),
    )
    return jax.shard_map(
        body,
        mesh=mesh,
        in_specs=placed,
        out_specs=(P("fs", None, "tp"), P("fs", None, "tp"), P("fs", None, "tp"), P("fs", "tp")),
        check_vma=False,
    )
```

profile of v0, /device:TPU:5, one launch (start us, length us, event | category | flops | bytes accessed | tf_op | source)
XLA Modules:
  0.0 257.7 jit_solution(10696394020961575395)
XLA Ops:
  0.7 1.9 convert_element_type.56
  2.6 0.3 copy-done.3
  2.9 2.1 multiply_convert_fusion.1
  5.0 2.1 pad_maximum_fusion
  7.1 5.7 %all-to-all-start = ((bf16[8,512,384]{2,1,0:T(8,128)(2,1)}), bf16[8,512,384]{2,1,0:T(8,128)(2,1)S(1)}, u32[]{:S(2)}, u32[]{:S(2)}) async-start(bf16[8,512,384]{2,1,0:T(8,128)(2,1)} %pad_maximum_fusion), calls=%async_computation | async-start | bytes 6291456 | tf_op jit(solution)/shard_map/all_to_all | solution.py:46
  12.8 1.4 fusion.1
  14.1 6.0 %psum.7 = f32[384]{0:T(512)S(1)} all-reduce(f32[384]{0:T(512)S(1)} %fusion.1), channel_id=1, replica_groups=mesh['fs'=8,'tp'=4] {'tp'}, use_global_device_ids=true, to_apply=%region_6.7 | all-reduce | flops 384 | bytes 3072 | tf_op jit(solution)/shard_map/psum | solution.py:53
  20.4 0.6 fusion
  21.0 3.1 %convolution_convert_fusion = bf16[1536,1024]{1,0:T(8,128)(2,1)S(1)} fusion(pred[384,1536]{1,0:T(8,128)(4,1)S(1)} %fusion, bf16[384,1024]{1,0:T(8,128)(2,1)} %param.7, f32[384]{0:T(512)S(1)} %add_rsqrt_fusion), kind=kOutput, calls=%fused_computation.3 | convolution fusion | flops 1210712064 | bytes 4523520 | tf_op jit(solution)/shard_map/dot_general | solution.py:70
  24.1 2.0 fusion.56
  26.0 56.6 %all-to-all-done = bf16[8,512,384]{2,1,0:T(8,128)(2,1)S(1)} async-done(((bf16[8,512,384]{2,1,0:T(8,128)(2,1)}), bf16[8,512,384]{2,1,0:T(8,128)(2,1)S(1)}, u32[]{:S(2)}, u32[]{:S(2)}) %all-to-all-start) | async-done | bytes 3145760 | tf_op jit(solution)/shard_map/all_to_all | solution.py:46
  82.7 4.6 %all-to-all-start.1 = ((bf16[8,96,1024]{2,1,0:T(8,128)(2,1)}), bf16[8,96,1024]{2,1,0:T(8,128)(2,1)}, u32[]{:S(2)}, u32[]{:S(2)}) async-start(bf16[8,96,1024]{2,1,0:T(8,128)(2,1)} %bitcast.62), calls=%async_computation.1 | async-start | bytes 3145728 | tf_op jit(solution)/shard_map/all_to_all | solution.py:89
  87.4 1.1 constant_dynamic-slice_fusion
  88.8 23.1 %collective-permute-done = bf16[2048,256]{1,0:T(8,128)(2,1)} collective-permute-done((bf16[2048,256]{1,0:T(8,128)(2,1)S(1)}, bf16[2048,256]{1,0:T(8,128)(2,1)}, u32[]{:S(2)}, u32[]{:S(2)}) %collective-permute-start) | collective-permute-done | bytes 1048608 | tf_op jit(solution)/shard_map/ppermute | solution.py:79
  111.9 11.3 %all-to-all-done.1 = bf16[8,96,1024]{2,1,0:T(8,128)(2,1)} async-done(((bf16[8,96,1024]{2,1,0:T(8,128)(2,1)}), bf16[8,96,1024]{2,1,0:T(8,128)(2,1)}, u32[]{:S(2)}, u32[]{:S(2)}) %all-to-all-start.1) | async-done | bytes 1572896 | tf_op jit(solution)/shard_map/all_to_all | solution.py:89
  123.2 2.2 collective-permute-start.1
  125.4 4.3 %all-to-all-start.2 = ((bf16[8,96,1024]{2,1,0:T(8,128)(2,1)}), bf16[8,96,1024]{2,1,0:T(8,128)(2,1)}, u32[]{:S(2)}, u32[]{:S(2)}) async-start(bf16[8,96,1024]{2,1,0:T(8,128)(2,1)} %bitcast.61), calls=%async_computation.2 | async-start | bytes 3145728 | tf_op jit(solution)/shard_map/all_to_all | solution.py:89
  129.7 2.1 fusion.23
  131.8 2.9 %fusion.5 = bf16[768,256]{0,1:T(8,128)(2,1)} fusion(f32[768,256]{0,1:T(8,128)S(1)} %fusion.23, bf16[768,1024]{1,0:T(8,128)(2,1)} %bitcast.4, bf16[2,1024,256]{2,1,0:T(8,128)(2,1)} %bitcast.8, s32[]{:T(128)S(6)} %select_n.101), kind=kOutput, calls=%fused_computation.20 | convolution fusion | flops 403046400 | bytes 3276804 | tf_op jit(solution)/shard_map/dot_general | solution.py:118
  135.0 2.2 fusion.29
  137.2 8.5 %collective-permute-done.2 = bf16[768,256]{0,1:T(8,128)(2,1)S(1)} collective-permute-done((bf16[768,256]{0,1:T(8,128)(2,1)}, bf16[768,256]{0,1:T(8,128)(2,1)S(1)}, u32[]{:S(2)}, u32[]{:S(2)}) %collective-permute-start.2) | collective-permute-done | bytes 393248 | tf_op jit(solution)/shard_map/ppermute | solution.py:121
  145.7 2.0 fusion.4
  148.2 1.9 fusion.57
  150.0 3.7 %collective-permute-done.3 = bf16[768,128]{0,1:T(8,128)(2,1)S(1)} collective-permute-done((bf16[768,128]{0,1:T(8,128)(2,1)S(1)}, bf16[768,128]{0,1:T(8,128)(2,1)S(1)}, u32[]{:S(2)}, u32[]{:S(2)}) %collective-permute-start.3) | collective-permute-done | bytes 196640 | tf_op jit(solution)/shard_map/ppermute | solution.py:124
  153.8 1.6 collective-permute-start.4
  155.7 0.5 collective-permute-start.6
  156.1 1.3 collective-permute-start.5
  157.4 7.1 %collective-permute-done.7 = bf16[1024,128]{1,0:T(8,128)(2,1)S(1)} collective-permute-done((bf16[1024,128]{1,0:T(8,128)(2,1)S(1)}, bf16[1024,128]{1,0:T(8,128)(2,1)S(1)}, u32[]{:S(2)}, u32[]{:S(2)}) %collective-permute-start.7) | collective-permute-done | bytes 262176 | tf_op jit(solution)/shard_map/ppermute | solution.py:107
  164.5 4.2 %collective-permute-done.5 = bf16[1024,128]{1,0:T(8,128)(2,1)S(1)} collective-permute-done((bf16[1024,128]{1,0:T(8,128)(2,1)S(1)}, bf16[1024,128]{1,0:T(8,128)(2,1)S(1)}, u32[]{:S(2)}, u32[]{:S(2)}) %collective-permute-start.5) | collective-permute-done | bytes 262176 | tf_op jit(solution)/shard_map/ppermute | solution.py:107
  168.7 2.2 convolution_convert_fusion.2
  170.9 1.1 collective-permute-start.8
  172.1 5.1 %all-to-all-start.3 = ((bf16[8,96,1024]{2,1,0:T(8,128)(2,1)}), bf16[8,96,1024]{2,1,0:T(8,128)(2,1)}, u32[]{:S(2)}, u32[]{:S(2)}) async-start(bf16[8,96,1024]{2,1,0:T(8,128)(2,1)} %bitcast.64), calls=%async_computation.3 | async-start | bytes 3145728 | tf_op jit(solution)/shard_map/all_to_all | solution.py:139
  177.1 2.1 fusion.25
  179.3 1.8 fusion.6
  181.0 0.3 collective-permute-start.9
  181.3 2.0 fusion.31
  183.4 8.2 %collective-permute-done.9 = bf16[768,256]{0,1:T(8,128)(2,1)S(1)} collective-permute-done((bf16[768,256]{0,1:T(8,128)(2,1)S(1)}, bf16[768,256]{0,1:T(8,128)(2,1)S(1)}, u32[]{:S(2)}, u32[]{:S(2)}) %collective-permute-start.9) | collective-permute-done | bytes 393248 | tf_op jit(solution)/shard_map/ppermute | solution.py:121
  191.6 0.6 fusion.3
  192.7 5.3 %collective-permute-done.10 = bf16[768,128]{0,1:T(8,128)(2,1)S(1)} collective-permute-done((bf16[768,128]{0,1:T(8,128)(2,1)S(1)}, bf16[768,128]{0,1:T(8,128)(2,1)S(1)}, u32[]{:S(2)}, u32[]{:S(2)}) %collective-permute-start.10) | collective-permute-done | bytes 196640 | tf_op jit(solution)/shard_map/ppermute | solution.py:124
  198.0 1.9 collective-permute-start.11
  199.9 1.3 collective-permute-done.11
  201.2 2.2 convolution_convert_fusion.1
  203.4 10.6 %all-to-all-done.3 = bf16[8,96,1024]{2,1,0:T(8,128)(2,1)} async-done(((bf16[8,96,1024]{2,1,0:T(8,128)(2,1)}), bf16[8,96,1024]{2,1,0:T(8,128)(2,1)}, u32[]{:S(2)}, u32[]{:S(2)}) %all-to-all-start.3) | async-done | bytes 1572896 | tf_op jit(solution)/shard_map/all_to_all | solution.py:139
  214.0 4.2 %all-to-all-start.4 = ((bf16[8,96,1024]{2,1,0:T(8,128)(2,1)}), bf16[8,96,1024]{2,1,0:T(8,128)(2,1)S(1)}, u32[]{:S(2)}, u32[]{:S(2)}) async-start(bf16[8,96,1024]{2,1,0:T(8,128)(2,1)} %bitcast.19), calls=%async_computation.4 | async-start | bytes 3145728 | tf_op jit(solution)/shard_map/all_to_all | solution.py:141
  218.3 0.6 select_reduce_fusion
  218.9 3.3 %fusion.20 = f32[384,1024]{1,0:T(8,128)} fusion(bf16[768,1024]{1,0:T(8,128)(2,1)} %bitcast.17, bf16[384,1536]{1,0:T(8,128)(2,1)S(1)} %select_reduce_fusion), kind=kOutput, calls=%fused_computation.37 | convolution fusion | flops 603979776 | bytes 3735552 | tf_op jit(solution)/shard_map/dot_general | solution.py:147
  222.2 32.4 %all-to-all-done.4 = bf16[8,96,1024]{2,1,0:T(8,128)(2,1)S(1)} async-done(((bf16[8,96,1024]{2,1,0:T(8,128)(2,1)}), bf16[8,96,1024]{2,1,0:T(8,128)(2,1)S(1)}, u32[]{:S(2)}, u32[]{:S(2)}) %all-to-all-start.4) | async-done | bytes 1572896 | tf_op jit(solution)/shard_map/all_to_all | solution.py:141
  254.6 3.1 %add_convert_fusion = bf16[384,1024]{1,0:T(8,128)(2,1)} fusion(f32[384,1024]{1,0:T(8,128)} %fusion.20, bf16[768,1024]{1,0:T(8,128)(2,1)S(1)} %bitcast.60, bf16[384,1536]{1,0:T(8,128)(2,1)S(1)} %select_reduce_fusion), kind=kOutput, calls=%fused_computation.13 | convolution fusion | flops 604766208 | bytes 4521984 | tf_op jit(solution)/shard_map/dot_general | solution.py:147
  (48 shorter events, 2.0 us)
Async XLA Ops:
  0.6 2.2 copy-start.3
  0.6 2.2 copy-start.6
  7.1 13.0 %copy-start.4 = (s32[384,2]{0,1:T(2,128)S(1)}, s32[384,2]{0,1:T(2,128)}, u32[]{:S(2)}) copy-start(s32[384,2]{0,1:T(2,128)} %param.12) | copy-start | bytes 9220
  7.1 75.6 %all-to-all-start = ((bf16[8,512,384]{2,1,0:T(8,128)(2,1)}), bf16[8,512,384]{2,1,0:T(8,128)(2,1)S(1)}, u32[]{:S(2)}, u32[]{:S(2)}) async-start(bf16[8,512,384]{2,1,0:T(8,128)(2,1)} %pad_maximum_fusion), calls=%async_computation | async-start | bytes 6291456 | tf_op jit(solution)/shard_map/all_to_all | solution.py:46
  82.7 40.5 %all-to-all-start.1 = ((bf16[8,96,1024]{2,1,0:T(8,128)(2,1)}), bf16[8,96,1024]{2,1,0:T(8,128)(2,1)}, u32[]{:S(2)}, u32[]{:S(2)}) async-start(bf16[8,96,1024]{2,1,0:T(8,128)(2,1)} %bitcast.62), calls=%async_computation.1 | async-start | bytes 3145728 | tf_op jit(solution)/shard_map/all_to_all | solution.py:89
  88.6 23.3 %collective-permute-start = (bf16[2048,256]{1,0:T(8,128)(2,1)S(1)}, bf16[2048,256]{1,0:T(8,128)(2,1)}, u32[]{:S(2)}, u32[]{:S(2)}) collective-permute-start(bf16[2048,256]{1,0:T(8,128)(2,1)S(1)} %get-tuple-element.22), channel_id=1, source_target_pairs={{0,2},{1,3},{2,0},{3,1},{4,6},{5,7},{6,4},{7,5},{8,10},{9,11},{10,... | collective-permute-start | bytes 3145736 | tf_op jit(solution)/shard_map/ppermute | solution.py:79
  123.2 6.5 %collective-permute-start.1 = (bf16[768,1024]{1,0:T(8,128)(2,1)}, bf16[768,1024]{1,0:T(8,128)(2,1)}, u32[]{:S(2)}, u32[]{:S(2)}) collective-permute-start(bf16[768,1024]{1,0:T(8,128)(2,1)} %bitcast.4), channel_id=1, source_target_pairs={{0,1},{1,0},{2,3},{3,2},{4,5},{5,4},{6,7},{7,6},{8,9},{9,8},{10,11... | collective-permute-start | bytes 4718600 | tf_op jit(solution)/shard_map/ppermute | solution.py:113
  125.4 45.6 %all-to-all-start.2 = ((bf16[8,96,1024]{2,1,0:T(8,128)(2,1)}), bf16[8,96,1024]{2,1,0:T(8,128)(2,1)}, u32[]{:S(2)}, u32[]{:S(2)}) async-start(bf16[8,96,1024]{2,1,0:T(8,128)(2,1)} %bitcast.61), calls=%async_computation.2 | async-start | bytes 3145728 | tf_op jit(solution)/shard_map/all_to_all | solution.py:89
  134.7 11.0 %collective-permute-start.2 = (bf16[768,256]{0,1:T(8,128)(2,1)}, bf16[768,256]{0,1:T(8,128)(2,1)S(1)}, u32[]{:S(2)}, u32[]{:S(2)}) collective-permute-start(bf16[768,256]{0,1:T(8,128)(2,1)} %fusion.5), channel_id=1, source_target_pairs={{0,2},{1,3},{2,0},{3,1},{4,6},{5,7},{6,4},{7,5},{8,10},{9,11},{10,... | collective-permute-start | bytes 1179656 | tf_op jit(solution)/shard_map/ppermute | solution.py:121
  135.0 10.8 %copy-start = (bf16[1,2048,256]{2,1,0:T(8,128)(2,1)S(1)}, bf16[1,2048,256]{2,1,0:T(8,128)(2,1)}, u32[]{:S(2)}) copy-start(bf16[1,2048,256]{2,1,0:T(8,128)(2,1)} %get-tuple-element.21) | copy-start | bytes 3145732
  147.9 5.9 %collective-permute-start.3 = (bf16[768,128]{0,1:T(8,128)(2,1)S(1)}, bf16[768,128]{0,1:T(8,128)(2,1)S(1)}, u32[]{:S(2)}, u32[]{:S(2)}) collective-permute-start(bf16[768,128]{0,1:T(8,128)(2,1)S(1)} %fusion.43), channel_id=1, source_target_pairs={{0,2},{1,3},{2,0},{3,1},{4,6},{5,7},{6,4},{7,5},{8,10},{9,11},{10,... | collective-permute-start | bytes 589832 | tf_op jit(solution)/shard_map/ppermute | solution.py:124
  150.0 5.3 %copy-start.2 = (bf16[1,4096,128]{2,1,0:T(8,128)(2,1)}, bf16[1,4096,128]{2,1,0:T(8,128)(2,1)S(1)}, u32[]{:S(2)}) copy-start(bf16[1,4096,128]{2,1,0:T(8,128)(2,1)S(1)} %get-tuple-element.18) | copy-start | bytes 3145732
  153.8 14.9 %collective-permute-start.4 = (bf16[768,256]{0,1:T(8,128)(2,1)S(1)}, bf16[768,256]{0,1:T(8,128)(2,1)S(1)}, u32[]{:S(2)}, u32[]{:S(2)}) collective-permute-start(bf16[768,256]{0,1:T(8,128)(2,1)S(1)} %pad_maximum_fusion.2), channel_id=1, source_target_pairs={{0,1},{1,0},{2,3},{3,2},{4,5},{5,4},{6,7},{7,6},{8,9},{9,8},{10,11... | collective-permute-start | bytes 1179656 | tf_op jit(solution)/shard_map/ppermute | solution.py:125
  155.5 9.1 %collective-permute-start.7 = (bf16[1024,128]{1,0:T(8,128)(2,1)S(1)}, bf16[1024,128]{1,0:T(8,128)(2,1)S(1)}, u32[]{:S(2)}, u32[]{:S(2)}) collective-permute-start(bf16[1024,128]{1,0:T(8,128)(2,1)S(1)} %get-tuple-element.24), channel_id=1, source_target_pairs={{0,3},{1,2},{2,1},{3,0},{4,7},{5,6},{6,5},{7,4},{8,11},{9,10},{10,... | collective-permute-start | bytes 786440 | tf_op jit(solution)/shard_map/ppermute | solution.py:107
  155.7 8.9 %collective-permute-start.6 = (bf16[1024,128]{1,0:T(8,128)(2,1)S(1)}, bf16[1024,128]{1,0:T(8,128)(2,1)S(1)}, u32[]{:S(2)}, u32[]{:S(2)}) collective-permute-start(bf16[1024,128]{1,0:T(8,128)(2,1)S(1)} %get-tuple-element.25), channel_id=1, source_target_pairs={{0,1},{1,0},{2,3},{3,2},{4,5},{5,4},{6,7},{7,6},{8,9},{9,8},{10,11... | collective-permute-start | bytes 786440 | tf_op jit(solution)/shard_map/ppermute | solution.py:107
  156.1 12.6 %collective-permute-start.5 = (bf16[1024,128]{1,0:T(8,128)(2,1)S(1)}, bf16[1024,128]{1,0:T(8,128)(2,1)S(1)}, u32[]{:S(2)}, u32[]{:S(2)}) collective-permute-start(bf16[1024,128]{1,0:T(8,128)(2,1)S(1)} %get-tuple-element.26), channel_id=1, source_target_pairs={{0,2},{1,3},{2,0},{3,1},{4,6},{5,7},{6,4},{7,5},{8,10},{9,11},{10,... | collective-permute-start | bytes 786440 | tf_op jit(solution)/shard_map/ppermute | solution.py:107
  164.5 6.4 %copy-start.7 = (bf16[1024,128]{1,0:T(8,128)(2,1)}, bf16[1024,128]{1,0:T(8,128)(2,1)S(1)}, u32[]{:S(2)}) copy-start(bf16[1024,128]{1,0:T(8,128)(2,1)S(1)} %collective-permute-done.7) | copy-start | bytes 786436
  164.5 6.4 %copy-start.9 = (bf16[1024,128]{1,0:T(8,128)(2,1)}, bf16[1024,128]{1,0:T(8,128)(2,1)S(1)}, u32[]{:S(2)}) copy-start(bf16[1024,128]{1,0:T(8,128)(2,1)S(1)} %collective-permute-done.6) | copy-start | bytes 786436
  168.7 2.2 copy-start.11
  170.9 8.3 %collective-permute-start.8 = (bf16[768,1024]{1,0:T(8,128)(2,1)}, bf16[768,1024]{1,0:T(8,128)(2,1)S(1)}, u32[]{:S(2)}, u32[]{:S(2)}) collective-permute-start(bf16[768,1024]{1,0:T(8,128)(2,1)} %bitcast.18), channel_id=1, source_target_pairs={{0,1},{1,0},{2,3},{3,2},{4,5},{5,4},{6,7},{7,6},{8,9},{9,8},{10,11... | collective-permute-start | bytes 4718600 | tf_op jit(solution)/shard_map/ppermute | solution.py:113
  172.1 42.0 %all-to-all-start.3 = ((bf16[8,96,1024]{2,1,0:T(8,128)(2,1)}), bf16[8,96,1024]{2,1,0:T(8,128)(2,1)}, u32[]{:S(2)}, u32[]{:S(2)}) async-start(bf16[8,96,1024]{2,1,0:T(8,128)(2,1)} %bitcast.64), calls=%async_computation.3 | async-start | bytes 3145728 | tf_op jit(solution)/shard_map/all_to_all | solution.py:139
  179.3 2.1 copy-start.1
  181.0 10.5 %collective-permute-start.9 = (bf16[768,256]{0,1:T(8,128)(2,1)S(1)}, bf16[768,256]{0,1:T(8,128)(2,1)S(1)}, u32[]{:S(2)}, u32[]{:S(2)}) collective-permute-start(bf16[768,256]{0,1:T(8,128)(2,1)S(1)} %fusion.6), channel_id=1, source_target_pairs={{0,2},{1,3},{2,0},{3,1},{4,6},{5,7},{6,4},{7,5},{8,10},{9,11},{10,... | collective-permute-start | bytes 1179656 | tf_op jit(solution)/shard_map/ppermute | solution.py:121
  192.2 9.0 %copy-start.8 = (bf16[1024,128]{1,0:T(8,128)(2,1)S(1)}, bf16[1024,128]{1,0:T(8,128)(2,1)}, u32[]{:S(2)}) copy-start(bf16[1024,128]{1,0:T(8,128)(2,1)} %copy-done.7) | copy-start | bytes 786436
  192.2 9.0 %copy-start.10 = (bf16[1024,128]{1,0:T(8,128)(2,1)S(1)}, bf16[1024,128]{1,0:T(8,128)(2,1)}, u32[]{:S(2)}) copy-start(bf16[1024,128]{1,0:T(8,128)(2,1)} %copy-done.9) | copy-start | bytes 786436
  192.3 9.0 %copy-start.12 = (bf16[1024,128]{1,0:T(8,128)(2,1)S(1)}, bf16[1024,128]{1,0:T(8,128)(2,1)}, u32[]{:S(2)}) copy-start(bf16[1024,128]{1,0:T(8,128)(2,1)} %copy-done.11) | copy-start | bytes 786436
  192.4 5.6 %collective-permute-start.10 = (bf16[768,128]{0,1:T(8,128)(2,1)S(1)}, bf16[768,128]{0,1:T(8,128)(2,1)S(1)}, u32[]{:S(2)}, u32[]{:S(2)}) collective-permute-start(bf16[768,128]{0,1:T(8,128)(2,1)S(1)} %fusion.42), channel_id=1, source_target_pairs={{0,2},{1,3},{2,0},{3,1},{4,6},{5,7},{6,4},{7,5},{8,10},{9,11},{10,... | collective-permute-start | bytes 589832 | tf_op jit(solution)/shard_map/ppermute | solution.py:124
  198.0 3.2 %collective-permute-start.11 = (bf16[768,256]{0,1:T(8,128)(2,1)S(1)}, bf16[768,256]{0,1:T(8,128)(2,1)S(1)}, u32[]{:S(2)}, u32[]{:S(2)}) collective-permute-start(bf16[768,256]{0,1:T(8,128)(2,1)S(1)} %pad_maximum_fusion.3), channel_id=1, source_target_pairs={{0,1},{1,0},{2,3},{3,2},{4,5},{5,4},{6,7},{7,6},{8,9},{9,8},{10,11... | collective-permute-start | bytes 1179656 | tf_op jit(solution)/shard_map/ppermute | solution.py:125
  214.0 4.2 %copy-start.5 = (f32[384,2]{0,1:T(2,128)S(1)}, f32[384,2]{0,1:T(2,128)}, u32[]{:S(2)}) copy-start(f32[384,2]{0,1:T(2,128)} %param.13) | copy-start | bytes 9220
  214.0 40.6 %all-to-all-start.4 = ((bf16[8,96,1024]{2,1,0:T(8,128)(2,1)}), bf16[8,96,1024]{2,1,0:T(8,128)(2,1)S(1)}, u32[]{:S(2)}, u32[]{:S(2)}) async-start(bf16[8,96,1024]{2,1,0:T(8,128)(2,1)} %bitcast.19), calls=%async_computation.4 | async-start | bytes 3145728 | tf_op jit(solution)/shard_map/all_to_all | solution.py:141
where the time goes:
time: 261 us; the launch traced here: 258 us
  waiting for transfers between devices  173 us (66%)
  starting transfers between devices  33.8 us (13%)
  matrix products  29.8 us (11%)
  other arithmetic  9.17 us (4%)
  blocking collectives  5.97 us (2%)
  local copies, waits for them, and re-layouts  5.49 us (2%)
    all_to_all x1, waiting for transfers between devices, body(): trio = lax.all_to_all(trio, 'fs', split_axis=0, concat_axis=1, tiled=True)  56.6 us
    all_to_all x2, waiting for transfers between devices, body(): lax.all_to_all(served, 'fs', split_axis=0, concat_axis=0, tiled=True)  43 us
    ppermute x1, waiting for transfers between devices, body(): lax.ppermute(lax.dynamic_slice_in_dim(pair[0], (1 - my_half) * span, span...  23.1 us
    ppermute x2, waiting for transfers between devices, serve(): lax.ppermute(partial(partner_blocks).astype(jnp.bfloat16), 'tp', cross_sw...  16.8 us
    dot_general x8, matrix products, partial(): total = total + jnp.dot(piece, block, preferred_element_type=jnp.float32)  15.8 us
    ppermute x3, waiting for transfers between devices, body(): piece = lax.ppermute(piece, 'tp', member_shift(j, crossed, n_tp))  11.3 us
    all_to_all x2, waiting for transfers between devices, body(): last = lax.all_to_all(ready, 'fs', split_axis=0, concat_axis=0, tiled=True)  11.3 us
    all_to_all x2, starting transfers between devices, body(): lax.all_to_all(served, 'fs', split_axis=0, concat_axis=0, tiled=True)  9.24 us
  transfers between devices with their start and end apart: 17, of which 12 were waited for; matrix products, arithmetic and copies ran while one was open for 14% of the time, Pallas kernels for 0%

commit v1 on v0

--- a/solution.py
+++ b/solution.py
@@ -1,6 +1,10 @@
+import functools
+
 import jax
 import jax.numpy as jnp
 from jax import lax
+from jax.experimental import pallas as pl
+from jax.experimental.pallas import tpu as pltpu
 from jax.sharding import PartitionSpec as P
 
 norm_eps = 1e-06
@@ -22,7 +26,7 @@
     ]
 
 
-def body(tokens, gate_master, up_master, down_master, norm_gain, routes, route_weight):
+def plain_body(tokens, gate_master, up_master, down_master, norm_gain, routes, route_weight):
     n_experts = gate_master.shape[0]
     tok_rows, top_count = routes.shape
     capacity = 2 * tok_rows * top_count // n_experts
@@ -148,6 +152,520 @@
     return (gate_out, up_out, down_out, mixed.astype(jnp.bfloat16))
 
 
+PAIR = 2
+VMEM_BUDGET = 62 * 1024 * 1024
+
+
+def near_first(n_z):
+    return [sorted(range(n_z), key=lambda b: (abs(b - z), b)) for z in range(n_z)]
+
+
+def far_first(n_z):
+    def rank(z, b):
+        return (-abs(b - z), min(b, n_z - 1 - b), b)
+
+    return [sorted(range(n_z), key=lambda b: rank(z, b)) for z in range(n_z)]
+
+
+def looked_up(table, z, step):
+    chosen = 0
+    for i, row in enumerate(table):
+        for s, value in enumerate(row):
+            chosen = chosen + jnp.where((z == i) & (step == s), value, 0)
+    return chosen
+
+
+def moe_kernel(
+    dims,
+    tok, gain, routes, weight, gate_hbm, up_hbm, down_hbm,
+    gate_out, up_out, down_out, mixed_out,
+    stage, wgu_send, wd_send, wgu_recv, wd_recv, blk, rows, xsend, hid, dn, yb, ysend,
+    rs_send, rs_recv, acc, ssq, aux_send, aux_recv, gain_mat,
+    stage_sem, ssq_s, ssq_r, aux_s, aux_r, ag_sr, ag_sl, ag_r,
+    wgu_s, wgu_r, wd_s, wd_r, x_s, x_r,
+    rc_s, rc_r, ry_s, ry_r, rf_s, rf_r,
+    hc_s, hc_r, hy_s, hy_r, hf_s, hf_r,
+    dn_s, dn_r, y_s, y_r, rs_sr, rs_sl, rs_r, out_sem,
+):
+    n_fs, n_tp, n_z, r_rows, feat, d_loc, h_cols, cap = dims
+    top_count = routes.shape[0]
+    f32, bf16 = jnp.float32, jnp.bfloat16
+    me = lax.axis_index("fs")
+    t = lax.axis_index("tp")
+    z, x = me // PAIR, me % PAIR
+    xp = me - x + (1 - x)
+    half = n_tp // 2
+    tc = (t // half) * half + (half - 1 - t % half)
+    ty = (t + half) % n_tp
+    near, far = near_first(n_z), far_first(n_z)
+    per_quarter = feat // d_loc
+
+    def remote(src, dst, ssem, rsem, **where):
+        return pltpu.make_async_remote_copy(
+            src_ref=src, dst_ref=dst, send_sem=ssem, recv_sem=rsem,
+            device_id=where, device_id_type=pl.DeviceIdType.MESH,
+        )
+
+    masters = (gate_hbm, up_hbm, down_hbm)
+
+    def load(i, e):
+        return pltpu.make_async_copy(masters[i].at[e], stage.at[i, e], stage_sem.at[i, e])
+
+    def every(count, body):
+        def step(i, carry):
+            body(i)
+            return carry
+        lax.fori_loop(0, count, step, 0)
+
+    barrier = pltpu.get_barrier_semaphore()
+    for d in range(1, n_fs):
+        pl.semaphore_signal(barrier, inc=1, device_id={"fs": (me + d) % n_fs},
+                            device_id_type=pl.DeviceIdType.MESH)
+    for d in range(1, n_tp):
+        pl.semaphore_signal(barrier, inc=1, device_id={"tp": (t + d) % n_tp},
+                            device_id_type=pl.DeviceIdType.MESH)
+
+    def start_load(d):
+        for i in range(3):
+            load(i, (me + d) % n_fs).start()
+    every(n_fs, start_load)
+
+    value = tok[...].astype(f32)
+    column = jnp.sum(value * value, axis=1, keepdims=True)
+    spread = jnp.transpose(jnp.broadcast_to(column, (r_rows, 128)))
+    ssq[t] = spread[:8]
+
+    pl.semaphore_wait(barrier, n_fs - 1 + n_tp - 1)
+
+    def ssq_copy(d):
+        peer = (t + d) % n_tp
+        return remote(ssq.at[t], ssq.at[t], ssq_s.at[d], ssq_r.at[t], tp=peer)
+
+    def ssq_from(d):
+        peer = (t + n_tp - d) % n_tp
+        return remote(ssq.at[peer], ssq.at[peer], ssq_s.at[d], ssq_r.at[peer], tp=peer)
+    for d in range(1, n_tp):
+        ssq_copy(d).start()
+
+    expert = lax.broadcasted_iota(jnp.int32, (n_fs, r_rows), 0)
+    picks = [jnp.broadcast_to(routes[k : k + 1, :], (n_fs, r_rows)) == expert for k in range(top_count)]
+    weights = weight[...]
+    mix = weights / jnp.sum(weights, axis=0, keepdims=True)
+    named = jnp.zeros((n_fs, r_rows), f32)
+    mixed_t = jnp.zeros((n_fs, r_rows), f32)
+    for k in range(top_count):
+        named = named + jnp.where(picks[k], 1.0, 0.0)
+        mixed_t = mixed_t + jnp.where(picks[k], jnp.broadcast_to(mix[k : k + 1, :], (n_fs, r_rows)), 0.0)
+    first = lax.broadcasted_iota(jnp.int32, (r_rows, r_rows), 0)
+    second = lax.broadcasted_iota(jnp.int32, (r_rows, r_rows), 1)
+    earlier = jnp.where(first < second, 1.0, 0.0).astype(bf16)
+    before = jnp.dot(named.astype(bf16), earlier, preferred_element_type=f32)
+    slot_t = jnp.where(named > 0.0, before, -1.0)
+    for plane in range(n_z):
+        lo = plane * PAIR
+        aux_send[plane, 0:PAIR, :] = slot_t[lo : lo + PAIR]
+        aux_send[plane, PAIR : 2 * PAIR, :] = mixed_t[lo : lo + PAIR]
+        aux_send[plane, 2 * PAIR :, :] = jnp.zeros((8 - 2 * PAIR, r_rows), f32)
+    aux_recv[z] = aux_send[z]
+
+    def aux_copy(d):
+        plane = (z + d) % n_z
+        return remote(aux_send.at[plane], aux_recv.at[z], aux_s.at[d], aux_r.at[z], fs=plane * PAIR + x)
+
+    def aux_from(plane):
+        return remote(aux_send.at[plane], aux_recv.at[plane], aux_s.at[0], aux_r.at[plane], fs=me)
+    for d in range(1, n_z):
+        aux_copy(d).start()
+
+    gain_mat[...] = jnp.transpose(jnp.broadcast_to(gain[...], (h_cols, d_loc)))
+
+    def wgu_copy(d):
+        e = (me + d) % n_fs
+        return remote(wgu_send.at[e], wgu_recv.at[me], wgu_s.at[d], wgu_r.at[me], fs=e)
+
+    def wgu_from(j):
+        return remote(wgu_send.at[j], wgu_recv.at[j], wgu_s.at[0], wgu_r.at[j], fs=me)
+
+    def wd_copy(d):
+        e = (me + d) % n_fs
+        return remote(wd_send.at[e], wd_recv.at[me], wd_s.at[d], wd_r.at[me], fs=e)
+
+    def wd_from(j):
+        return remote(wd_send.at[j], wd_recv.at[j], wd_s.at[0], wd_r.at[j], fs=me)
+
+    def cast_gu(d, target, index):
+        e = (me + d) % n_fs
+        load(0, e).wait()
+        load(1, e).wait()
+        target[index, :, 0:h_cols] = (stage[0, e] * gain_mat[...]).astype(bf16)
+        target[index, :, h_cols : 2 * h_cols] = (stage[1, e] * gain_mat[...]).astype(bf16)
+
+    def cast_d(d, target, index):
+        e = (me + d) % n_fs
+        load(2, e).wait()
+        target[index] = stage[2, e].astype(bf16)
+
+    def send_gu(d):
+        cast_gu(d, wgu_send, (me + d) % n_fs)
+        wgu_copy(d).start()
+
+    def send_d(d):
+        cast_d(d, wd_send, (me + d) % n_fs)
+        wd_copy(d).start()
+
+    def span(first_d, last_d, body):
+        every(last_d - first_d, lambda i: body(i + first_d))
+
+    for d in range(1, n_tp):
+        ssq_from(d).wait_recv()
+    total = ssq[0]
+    for k in range(1, n_tp):
+        total = total + ssq[k]
+    inverse = lax.rsqrt(total / (feat * n_tp) + norm_eps)
+    inverse = jnp.transpose(jnp.broadcast_to(inverse[0:1], (128, r_rows)))[:, 0:1]
+    blk[z] = (tok[...].astype(f32) * inverse).astype(bf16)
+
+    def ag_right(b):
+        return remote(blk.at[b], blk.at[b], ag_sr.at[b], ag_r.at[b], fs=me + PAIR)
+
+    def ag_left(b):
+        return remote(blk.at[b], blk.at[b], ag_sl.at[b], ag_r.at[b], fs=me - PAIR)
+
+    def goes_right(b):
+        return (b <= z) & (z < n_z - 1)
+
+    def goes_left(b):
+        return (b >= z) & (z > 0)
+
+    def picker(b, which):
+        slots = aux_recv[b, pl.ds(which, 1), :]
+        at = lax.broadcasted_iota(jnp.int32, (cap, r_rows), 0).astype(f32)
+        return at == jnp.broadcast_to(slots, (cap, r_rows))
+
+    def x_copy(b):
+        return remote(xsend.at[b], rows.at[t, b, pl.ds(cap, cap)], x_s.at[b], x_r.at[b], fs=xp)
+
+    def stage_a(s):
+        b = looked_up(near, z, s)
+
+        @pl.when(b != z)
+        def _():
+            ag_right(b).wait_recv()
+            aux_from(b).wait_recv()
+
+        @pl.when(goes_right(b))
+        def _():
+            ag_right(b).start()
+
+        @pl.when(goes_left(b))
+        def _():
+            ag_left(b).start()
+        theirs = jnp.where(picker(b, 1 - x), 1.0, 0.0).astype(bf16)
+        xsend[b] = jnp.dot(theirs, blk[b], preferred_element_type=f32).astype(bf16)
+        x_copy(b).start()
+        ours = jnp.where(picker(b, x), 1.0, 0.0).astype(bf16)
+        rows[t, b, 0:cap, :] = jnp.dot(ours, blk[b], preferred_element_type=f32).astype(bf16)
+
+    def rc_copy(b):
+        return remote(rows.at[t, b], rows.at[t, b], rc_s.at[b], rc_r.at[b], tp=tc)
+
+    def ry_copy(b):
+        return remote(rows.at[t, b], rows.at[t, b], ry_s.at[b], ry_r.at[b], tp=ty)
+
+    def rf_copy(b):
+        return remote(rows.at[ty, b], rows.at[ty, b], rf_s.at[b], rf_r.at[b], tp=tc)
+
+    def stage_b(s):
+        b = looked_up(near, z, s)
+        x_copy(b).wait_recv()
+        ry_copy(b).start()
+        rc_copy(b).start()
+
+    def stage_c(s):
+        b = looked_up(near, z, s)
+        ry_copy(b).wait_recv()
+        rf_copy(b).start()
+
+    stage_a(0)
+    span(1, 3, send_gu)
+    stage_b(0)
+    span(3, 5, send_gu)
+    stage_a(1)
+    span(5, 7, send_gu)
+    stage_c(0)
+    stage_b(1)
+    span(7, n_fs, send_gu)
+    span(1, 3, send_d)
+    stage_a(2)
+    stage_c(1)
+    stage_b(2)
+    span(3, 5, send_d)
+    stage_a(3)
+    span(5, n_fs, send_d)
+    stage_c(2)
+    stage_b(3)
+    cast_gu(0, wgu_recv, me)
+    cast_d(0, wd_recv, me)
+    stage_c(3)
+
+    def wait_gu(d):
+        wgu_from((me + n_fs - d) % n_fs).wait_recv()
+    span(1, n_fs, wait_gu)
+
+    def hc_copy(b):
+        return remote(hid.at[t, b], hid.at[t, b], hc_s.at[b], hc_r.at[b], tp=tc)
+
+    def hy_copy(b):
+        return remote(hid.at[t, b], hid.at[t, b], hy_s.at[b], hy_r.at[b], tp=ty)
+
+    def hf_copy(b):
+        return remote(hid.at[ty, b], hid.at[ty, b], hf_s.at[b], hf_r.at[b], tp=tc)
+
+    def stage_d(s):
+        b = looked_up(far, z, s)
+        rc_copy(b).wait_recv()
+        rf_copy(b).wait_recv()
+        both = jnp.zeros((2 * cap, 2 * h_cols), f32)
+        for j in range(n_fs):
+            lo = (j % per_quarter) * d_loc
+            both = both + jnp.dot(rows[j // per_quarter, b, :, lo : lo + d_loc], wgu_recv[j],
+                                  preferred_element_type=f32)
+        gates = both[:, 0:h_cols]
+        hid[t, b] = (gates / (1.0 + jnp.exp(-gates)) * both[:, h_cols:]).astype(bf16)
+        hy_copy(b).start()
+        hc_copy(b).start()
+    every(n_z, stage_d)
+
+    def out_copies(j):
+        at = pl.ds(pl.multiple_of(j * d_loc, d_loc), d_loc)
+        return [
+            pltpu.make_async_copy(wgu_recv.at[j, :, pl.ds(0, h_cols)], gate_out.at[at], out_sem.at[0, j]),
+            pltpu.make_async_copy(wgu_recv.at[j, :, pl.ds(h_cols, h_cols)], up_out.at[at], out_sem.at[1, j]),
+            pltpu.make_async_copy(wd_recv.at[j], down_out.at[at], out_sem.at[2, j]),
+        ]
+
+    def dn_copy(j):
+        q = j % per_quarter
+        return remote(wd_recv.at[j], dn.at[q, t], dn_s.at[j], dn_r.at[q, t], tp=j // per_quarter)
+
+    def dn_from(q, k):
+        return remote(wd_recv.at[0], dn.at[q, k], dn_s.at[0], dn_r.at[q, k], tp=t)
+
+    def pass_down(d):
+        j = (me + n_fs - d) % n_fs
+
+        @pl.when(d > 0)
+        def _():
+            wd_from(j).wait_recv()
+
+        @pl.when(j // per_quarter == t)
+        def _():
+            dn[j % per_quarter, t] = wd_recv[j]
+
+        @pl.when(j // per_quarter != t)
+        def _():
+            dn_copy(j).start()
+        for copy in out_copies(j):
+            copy.start()
+    every(n_fs, pass_down)
+
+    def stage_e(s):
+        b = looked_up(far, z, s)
+        hy_copy(b).wait_recv()
+        hf_copy(b).start()
+    every(n_z, stage_e)
+
+    def wait_dn(d):
+        k = (t + d) % n_tp
+        for q in range(per_quarter):
+            dn_from(q, k).wait_recv()
+    span(1, n_tp, wait_dn)
+
+    def y_copy(b):
+        return remote(ysend.at[b], yb.at[b, pl.ds(cap, cap)], y_s.at[b], y_r.at[b], fs=xp)
+
+    def stage_f(s):
+        b = looked_up(far, z, s)
+        hc_copy(b).wait_recv()
+        hf_copy(b).wait_recv()
+        units = jnp.concatenate([hid[k, b] for k in range(n_tp)], axis=1)
+        for q in range(per_quarter):
+            mat = jnp.concatenate([dn[q, k] for k in range(n_tp)], axis=1)
+            result = lax.dot_general(units, mat, (((1,), (1,)), ((), ())), preferred_element_type=f32)
+            result = result.astype(bf16)
+            lo = q * d_loc
+            ysend[b, :, lo : lo + d_loc] = result[cap:]
+            yb[b, 0:cap, lo : lo + d_loc] = result[:cap]
+        y_copy(b).start()
+    every(n_z, stage_f)
+
+    def rs_right(b):
+        return remote(rs_send.at[b], rs_recv.at[b], rs_sr.at[b], rs_r.at[b], fs=me + PAIR)
+
+    def rs_left(b):
+        at = jnp.where(b == z - 1, n_z, b)
+        return remote(rs_send.at[b], rs_recv.at[at], rs_sl.at[b], rs_r.at[at], fs=me - PAIR)
+
+    def rs_from(at):
+        return remote(rs_send.at[0], rs_recv.at[at], rs_sr.at[0], rs_r.at[at], fs=me)
+
+    def stage_g(s):
+        b = looked_up(far, z, s)
+        y_copy(b).wait_recv()
+
+        def share(which):
+            weights = jnp.broadcast_to(aux_recv[b, pl.ds(PAIR + which, 1), :], (cap, r_rows))
+            return jnp.where(picker(b, which), weights, 0.0).astype(bf16)
+        spreading = jnp.concatenate([share(x), share(1 - x)], axis=0)
+        acc[...] = lax.dot_general(spreading, yb[b], (((0,), (0,)), ((), ())), preferred_element_type=f32)
+
+        @pl.when(((b >= z) & (z > 0)) | ((b < z) & (z < n_z - 1)))
+        def _():
+            rs_from(b).wait_recv()
+            acc[...] += rs_recv[b].astype(f32)
+
+        @pl.when((b == z) & (z < n_z - 1))
+        def _():
+            rs_from(n_z).wait_recv()
+            acc[...] += rs_recv[n_z].astype(f32)
+
+        @pl.when(b != z)
+        def _():
+            rs_send[b] = acc[...].astype(bf16)
+
+        @pl.when(b > z)
+        def _():
+            rs_right(b).start()
+
+        @pl.when(b < z)
+        def _():
+            rs_left(b).start()
+
+        @pl.when(b == z)
+        def _():
+            mixed_out[...] = acc[...].astype(bf16)
+    every(n_z, stage_g)
+
+    for d in range(1, n_tp):
+        ssq_copy(d).wait_send()
+    for d in range(1, n_z):
+        aux_copy(d).wait_send()
+
+    def sent_w(d):
+        wgu_copy(d).wait_send()
+        wd_copy(d).wait_send()
+    span(1, n_fs, sent_w)
+
+    def sent_b(b):
+        @pl.when(goes_right(b))
+        def _():
+            ag_right(b).wait_send()
+
+        @pl.when(goes_left(b))
+        def _():
+            ag_left(b).wait_send()
+        for copy in (x_copy, rc_copy, ry_copy, rf_copy, hc_copy, hy_copy, hf_copy, y_copy):
+            copy(b).wait_send()
+
+        @pl.when(b > z)
+        def _():
+            rs_right(b).wait_send()
+
+        @pl.when(b < z)
+        def _():
+            rs_left(b).wait_send()
+    every(n_z, sent_b)
+
+    def sent_j(j):
+        @pl.when(j // per_quarter != t)
+        def _():
+            dn_copy(j).wait_send()
+        for copy in out_copies(j):
+            copy.wait()
+    every(n_fs, sent_j)
+
+
+def scratch_for(dims):
+    n_fs, n_tp, n_z, r_rows, feat, d_loc, h_cols, cap = dims
+    f32, bf16 = jnp.float32, jnp.bfloat16
+    per_quarter = feat // d_loc
+    buffers = [
+        ((3, n_fs, d_loc, h_cols), f32),
+        ((n_fs, d_loc, 2 * h_cols), bf16),
+        ((n_fs, d_loc, h_cols), bf16),
+        ((n_fs, d_loc, 2 * h_cols), bf16),
+        ((n_fs, d_loc, h_cols), bf16),
+        ((n_z, r_rows, feat), bf16),
+        ((n_tp, n_z, 2 * cap, feat), bf16),
+        ((n_z, cap, feat), bf16),
+        ((n_tp, n_z, 2 * cap, h_cols), bf16),
+        ((per_quarter, n_tp, d_loc, h_cols), bf16),
+        ((n_z, 2 * cap, feat), bf16),
+        ((n_z, cap, feat), bf16),
+        ((n_z, r_rows, feat), bf16),
+        ((n_z + 1, r_rows, feat), bf16),
+        ((r_rows, feat), f32),
+        ((n_tp, 8, r_rows), f32),
+        ((n_z, 8, r_rows), f32),
+        ((n_z, 8, r_rows), f32),
+        ((d_loc, h_cols), f32),
+    ]
+    sems = [
+        (3, n_fs), (n_tp,), (n_tp,), (n_z,), (n_z,), (n_z,), (n_z,), (n_z,),
+        (n_fs,), (n_fs,), (n_fs,), (n_fs,), (n_z,), (n_z,),
+        (n_z,), (n_z,), (n_z,), (n_z,), (n_z,), (n_z,),
+        (n_z,), (n_z,), (n_z,), (n_z,), (n_z,), (n_z,),
+        (n_fs,), (per_quarter, n_tp), (n_z,), (n_z,), (n_z,), (n_z,), (n_z + 1,), (3, n_fs),
+    ]
+    return buffers, sems
+
+
+def dims_of(tokens, gate_master, routes):
+    n_fs, n_tp = lax.axis_size("fs"), lax.axis_size("tp")
+    n_experts, d_loc, h_cols = gate_master.shape
+    r_rows, top_count = routes.shape
+    cap = 2 * r_rows * top_count // n_experts
+    return (n_fs, n_tp, n_fs // PAIR, r_rows, tokens.shape[1], d_loc, h_cols, cap)
+
+
+def fits(dims, n_experts, top_count):
+    n_fs, n_tp, n_z, r_rows, feat, d_loc, h_cols, cap = dims
+    if n_experts != n_fs or n_fs % PAIR or n_tp != 2 * PAIR or n_z != 2 * PAIR:
+        return False
+    if feat % d_loc or cap % 16 or h_cols % 128 or r_rows % 128 or d_loc % 128:
+        return False
+    total = 4 * r_rows * feat
+    for shape, kind in scratch_for(dims)[0]:
+        size = jnp.dtype(kind).itemsize
+        for extent in shape:
+            size = size * extent
+        total = total + size
+    return total < VMEM_BUDGET * 9 // 10
+
+
+def body(tokens, gate_master, up_master, down_master, norm_gain, routes, route_weight):
+    dims = dims_of(tokens, gate_master, routes)
+    if not fits(dims, gate_master.shape[0], routes.shape[1]):
+        return plain_body(tokens, gate_master, up_master, down_master, norm_gain, routes, route_weight)
+    n_fs, n_tp, n_z, r_rows, feat, d_loc, h_cols, cap = dims
+    buffers, sems = scratch_for(dims)
+    vmem, anywhere = pl.BlockSpec(memory_space=pltpu.VMEM), pl.BlockSpec(memory_space=pl.ANY)
+    matrix = jax.ShapeDtypeStruct((n_fs * d_loc, h_cols), jnp.bfloat16)
+    gate_out, up_out, down_out, mixed = pl.pallas_call(
+        functools.partial(moe_kernel, dims),
+        out_shape=(matrix, matrix, matrix, jax.ShapeDtypeStruct((r_rows, feat), jnp.bfloat16)),
+        in_specs=[vmem] * 4 + [anywhere] * 3,
+        out_specs=(anywhere, anywhere, anywhere, vmem),
+        scratch_shapes=[pltpu.VMEM(shape, kind) for shape, kind in buffers]
+        + [pltpu.SemaphoreType.DMA(shape) for shape in sems],
+        compiler_params=pltpu.CompilerParams(
+            collective_id=0, has_side_effects=True, vmem_limit_bytes=VMEM_BUDGET
+        ),
+        name="experts",
+    )(tokens, norm_gain[None, :], routes.T, route_weight.T, gate_master, up_master, down_master)
+    return (gate_out[None], up_out[None], down_out[None], mixed)
+
+
 def solution(mesh):
     placed = (
         P("fs", "tp"),

time: 261 us -> 246 us (0.943)
  the two profiles are of different devices: /device:TPU:5 before, /device:TPU:10 now
where the time goes in v1:
time: 246 us
  Pallas kernels  240 us (98%)
  local copies, waits for them, and re-layouts  5.24 us (2%)
    pallas_call x1, Pallas kernels, body(): pl.pallas_call(functools.partial(moe_kernel, dims), out_shape=(matrix, ma...  240 us
    unnamed x10, local copies, waits for them, and re-layouts  5.24 us

profile of v1, /device:TPU:10, one launch (start us, length us, event | category | flops | bytes accessed | tf_op | source)
XLA Modules:
  0.0 245.8 jit_solution(52801573967089019)
XLA Ops:
  0.6 239.9 %experts.1 = (bf16[4096,128]{1,0:T(8,128)(2,1)}, bf16[4096,128]{1,0:T(8,128)(2,1)}, bf16[4096,128]{1,0:T(8,128)(2,1)}, bf16[384,1024]{1,0:T(8,128)(2,1)}) custom-call(bf16[384,1024]{1,0:T(8,128)(2,1)} %tok.1, f32[1,512]{1,0:T(1,128)} %bitcast.11, s32[2,384]{1,0:T(2,128)} %bitcast.9, f32[2,384]{1,0:T(2,128)} %bitcast.10, f32[8,512,128]{2,1,0:T(8,128)} %gate_hbm.1, ...), custom_call_target="tpu_custom_call" | custom-call | tf_op jit(solution)/shard_map/experts/pallas_call | solution.py:654
  240.5 0.0 copy-start.1
  240.5 0.0 copy-start
  240.5 2.4 copy.15
  242.9 0.0 copy-done.1
  242.9 0.0 copy-start.2
  242.9 1.0 copy.16
  243.9 0.0 copy-done
  243.9 1.0 copy.17
  244.9 0.0 copy-done.2
  244.9 0.9 copy.18
Async XLA Ops:
  240.5 2.4 copy-start.1
  240.5 3.4 %copy-start = (bf16[4096,128]{1,0:T(8,128)(2,1)S(1)}, bf16[4096,128]{1,0:T(8,128)(2,1)}, u32[]{:S(2)}) copy-start(bf16[4096,128]{1,0:T(8,128)(2,1)} %get-tuple-element.10) | copy-start | bytes 3145732
  242.9 1.9 copy-start.2

commit v2 on v1

--- a/solution.py
+++ b/solution.py
@@ -230,12 +230,15 @@
             load(i, (me + d) % n_fs).start()
     every(n_fs, start_load)
 
+    blk[z] = tok[...]
+
     value = tok[...].astype(f32)
     column = jnp.sum(value * value, axis=1, keepdims=True)
     spread = jnp.transpose(jnp.broadcast_to(column, (r_rows, 128)))
     ssq[t] = spread[:8]
 
-    pl.semaphore_wait(barrier, n_fs - 1 + n_tp - 1)
+    with jax.named_scope("bar"):
+        pl.semaphore_wait(barrier, n_fs - 1 + n_tp - 1)
 
     def ssq_copy(d):
         peer = (t + d) % n_tp
@@ -246,6 +249,28 @@
         return remote(ssq.at[peer], ssq.at[peer], ssq_s.at[d], ssq_r.at[peer], tp=peer)
     for d in range(1, n_tp):
         ssq_copy(d).start()
+
+    def ag_right(b):
+        return remote(blk.at[b], blk.at[b], ag_sr.at[b], ag_r.at[b], fs=me + PAIR)
+
+    def ag_left(b):
+        return remote(blk.at[b], blk.at[b], ag_sl.at[b], ag_r.at[b], fs=me - PAIR)
+
+    def goes_right(b):
+        return (b <= z) & (z < n_z - 1)
+
+    def goes_left(b):
+        return (b >= z) & (z > 0)
+
+    def ag_start(b):
+        @pl.when(goes_right(b))
+        def _():
+            ag_right(b).start()
+
+        @pl.when(goes_left(b))
+        def _():
+            ag_left(b).start()
+    ag_start(z)
 
     expert = lax.broadcasted_iota(jnp.int32, (n_fs, r_rows), 0)
     picks = [jnp.broadcast_to(routes[k : k + 1, :], (n_fs, r_rows)) == expert for k in range(top_count)]
@@ -261,11 +286,18 @@
     earlier = jnp.where(first < second, 1.0, 0.0).astype(bf16)
     before = jnp.dot(named.astype(bf16), earlier, preferred_element_type=f32)
     slot_t = jnp.where(named > 0.0, before, -1.0)
+    with jax.named_scope("ssqwait"):
+        for d in range(1, n_tp):
+            ssq_from(d).wait_recv()
+    total = ssq[0]
+    for k in range(1, n_tp):
+        total = total + ssq[k]
+    inverse = lax.rsqrt(total / (feat * n_tp) + norm_eps)
     for plane in range(n_z):
         lo = plane * PAIR
         aux_send[plane, 0:PAIR, :] = slot_t[lo : lo + PAIR]
         aux_send[plane, PAIR : 2 * PAIR, :] = mixed_t[lo : lo + PAIR]
-        aux_send[plane, 2 * PAIR :, :] = jnp.zeros((8 - 2 * PAIR, r_rows), f32)
+        aux_send[plane, 2 * PAIR :, :] = inverse[2 * PAIR :]
     aux_recv[z] = aux_send[z]
 
     def aux_copy(d):
@@ -316,27 +348,6 @@
     def span(first_d, last_d, body):
         every(last_d - first_d, lambda i: body(i + first_d))
 
-    for d in range(1, n_tp):
-        ssq_from(d).wait_recv()
-    total = ssq[0]
-    for k in range(1, n_tp):
-        total = total + ssq[k]
-    inverse = lax.rsqrt(total / (feat * n_tp) + norm_eps)
-    inverse = jnp.transpose(jnp.broadcast_to(inverse[0:1], (128, r_rows)))[:, 0:1]
-    blk[z] = (tok[...].astype(f32) * inverse).astype(bf16)
-
-    def ag_right(b):
-        return remote(blk.at[b], blk.at[b], ag_sr.at[b], ag_r.at[b], fs=me + PAIR)
-
-    def ag_left(b):
-        return remote(blk.at[b], blk.at[b], ag_sl.at[b], ag_r.at[b], fs=me - PAIR)
-
-    def goes_right(b):
-        return (b <= z) & (z < n_z - 1)
-
-    def goes_left(b):
-        return (b >= z) & (z > 0)
-
     def picker(b, which):
         slots = aux_recv[b, pl.ds(which, 1), :]
         at = lax.broadcasted_iota(jnp.int32, (cap, r_rows), 0).astype(f32)
@@ -351,20 +362,18 @@
         @pl.when(b != z)
         def _():
             ag_right(b).wait_recv()
+            ag_start(b)
             aux_from(b).wait_recv()
-
-        @pl.when(goes_right(b))
-        def _():
-            ag_right(b).start()
-
-        @pl.when(goes_left(b))
-        def _():
-            ag_left(b).start()
-        theirs = jnp.where(picker(b, 1 - x), 1.0, 0.0).astype(bf16)
-        xsend[b] = jnp.dot(theirs, blk[b], preferred_element_type=f32).astype(bf16)
+        scale = jnp.broadcast_to(aux_recv[b, 2 * PAIR : 2 * PAIR + 1, :], (cap, r_rows))
+
+        def compact(which):
+            hit = picker(b, which)
+            factor = jnp.sum(jnp.where(hit, scale, 0.0), axis=1, keepdims=True)
+            taken = jnp.dot(jnp.where(hit, 1.0, 0.0).astype(bf16), blk[b], preferred_element_type=f32)
+            return (taken * factor).astype(bf16)
+        xsend[b] = compact(1 - x)
         x_copy(b).start()
-        ours = jnp.where(picker(b, x), 1.0, 0.0).astype(bf16)
-        rows[t, b, 0:cap, :] = jnp.dot(ours, blk[b], preferred_element_type=f32).astype(bf16)
+        rows[t, b, 0:cap, :] = compact(x)
 
     def rc_copy(b):
         return remote(rows.at[t, b], rows.at[t, b], rc_s.at[b], rc_r.at[b], tp=tc)
@@ -386,31 +395,107 @@
         ry_copy(b).wait_recv()
         rf_copy(b).start()
 
-    stage_a(0)
-    span(1, 3, send_gu)
-    stage_b(0)
-    span(3, 5, send_gu)
-    stage_a(1)
-    span(5, 7, send_gu)
-    stage_c(0)
-    stage_b(1)
-    span(7, n_fs, send_gu)
-    span(1, 3, send_d)
-    stage_a(2)
-    stage_c(1)
-    stage_b(2)
-    span(3, 5, send_d)
-    stage_a(3)
-    span(5, n_fs, send_d)
-    stage_c(2)
-    stage_b(3)
+    def plane_sends(plane, body):
+        for k in range(PAIR):
+            body((plane * PAIR + k + n_fs - me) % n_fs)
+
+    def side_sends(to_right, body):
+        for d in range(1, n_z):
+            if to_right:
+                @pl.when(z + d < n_z)
+                def _():
+                    plane_sends(z + d, body)
+            else:
+                @pl.when(z >= d)
+                def _():
+                    plane_sends(z - d, body)
+
+    def shorter_side(body):
+        right = z < n_z // 2
+
+        @pl.when(right)
+        def _():
+            side_sends(False, body)
+
+        @pl.when(~right)
+        def _():
+            side_sends(True, body)
+
+    inner = (z > 0) & (z < n_z - 1)
+
+    def partner_sends(body):
+        body((xp + n_fs - me) % n_fs)
+
+    def named(kind, s):
+        with jax.named_scope(kind + str(s)):
+            {"a": stage_a, "b": stage_b, "c": stage_c}[kind](s)
+
+    def run(*steps):
+        for step in steps:
+            if isinstance(step, str):
+                named(step[0], int(step[1]))
+            else:
+                with jax.named_scope("w"):
+                    step()
+
+    def toward(distance, body):
+        @pl.when(z < n_z // 2)
+        def _():
+            plane_sends(z + distance, body)
+
+        @pl.when(z >= n_z // 2)
+        def _():
+            plane_sends(z - distance, body)
+
+    def forwarded():
+        @pl.when(z < n_z // 2)
+        def _():
+            ag_left(z + 2).wait_send()
+
+        @pl.when(z >= n_z // 2)
+        def _():
+            ag_right(z - 2).wait_send()
+
+    def partner_all():
+        partner_sends(send_gu)
+        partner_sends(send_d)
+
+    def inner_second():
+        forwarded()
+        toward(2, send_gu)
+        shorter_side(send_gu)
+
+    def inner_third():
+        toward(1, send_d)
+        toward(2, send_d)
+        shorter_side(send_d)
+
+    def outer_first():
+        toward(1, send_gu)
+        toward(1, send_d)
+
+    def outer_third():
+        toward(2, send_d)
+        toward(3, send_d)
+
+    @pl.when(inner)
+    def _():
+        run("a0", partner_all, "b0", "a1", "a2", "b1", "c0", "a3", lambda: toward(1, send_gu),
+            "b2", "c1", inner_second, "b3", "c2", inner_third)
+
+    @pl.when(~inner)
+    def _():
+        run("a0", partner_all, "b0", "a1", outer_first, "b1", "c0", "a2", lambda: toward(2, send_gu),
+            "b2", "c1", "a3", lambda: toward(3, send_gu), "b3", "c2", outer_third)
     cast_gu(0, wgu_recv, me)
     cast_d(0, wd_recv, me)
-    stage_c(3)
+    with jax.named_scope("c3"):
+        stage_c(3)
 
     def wait_gu(d):
         wgu_from((me + n_fs - d) % n_fs).wait_recv()
-    span(1, n_fs, wait_gu)
+    with jax.named_scope("span_1_n_fs_wait_gu_"):
+        span(1, n_fs, wait_gu)
 
     def hc_copy(b):
         return remote(hid.at[t, b], hid.at[t, b], hc_s.at[b], hc_r.at[b], tp=tc)
@@ -434,7 +519,8 @@
         hid[t, b] = (gates / (1.0 + jnp.exp(-gates)) * both[:, h_cols:]).astype(bf16)
         hy_copy(b).start()
         hc_copy(b).start()
-    every(n_z, stage_d)
+    with jax.named_scope("every_n_z_stage_d_"):
+        every(n_z, stage_d)
 
     def out_copies(j):
         at = pl.ds(pl.multiple_of(j * d_loc, d_loc), d_loc)
@@ -451,10 +537,8 @@
     def dn_from(q, k):
         return remote(wd_recv.at[0], dn.at[q, k], dn_s.at[0], dn_r.at[q, k], tp=t)
 
-    def pass_down(d):
-        j = (me + n_fs - d) % n_fs
-
-        @pl.when(d > 0)
+    def pass_down(j):
+        @pl.when(j != me)
         def _():
             wd_from(j).wait_recv()
 
@@ -467,22 +551,34 @@
             dn_copy(j).start()
         for copy in out_copies(j):
             copy.start()
-    every(n_fs, pass_down)
+
+    def pass_planes(first_s, last_s):
+        def one(s):
+            plane = looked_up(near, z, s)
+            for k in range(PAIR):
+                pass_down(plane * PAIR + k)
+        span(first_s, last_s, one)
+    with jax.named_scope("pass_near"):
+        pass_planes(0, n_z // 2)
 
     def stage_e(s):
         b = looked_up(far, z, s)
         hy_copy(b).wait_recv()
         hf_copy(b).start()
-    every(n_z, stage_e)
+    with jax.named_scope("every_n_z_stage_e_"):
+        every(n_z, stage_e)
+    with jax.named_scope("pass_far"):
+        pass_planes(n_z // 2, n_z)
 
     def wait_dn(d):
         k = (t + d) % n_tp
         for q in range(per_quarter):
             dn_from(q, k).wait_recv()
-    span(1, n_tp, wait_dn)
-
-    def y_copy(b):
-        return remote(ysend.at[b], yb.at[b, pl.ds(cap, cap)], y_s.at[b], y_r.at[b], fs=xp)
+    with jax.named_scope("span_1_n_tp_wait_dn_"):
+        span(1, n_tp, wait_dn)
+
+    def y_copy(b, q):
+        return remote(ysend.at[b, q], yb.at[b, q, pl.ds(cap, cap)], y_s.at[b, q], y_r.at[b, q], fs=xp)
 
     def stage_f(s):
         b = looked_up(far, z, s)
@@ -493,58 +589,60 @@
             mat = jnp.concatenate([dn[q, k] for k in range(n_tp)], axis=1)
             result = lax.dot_general(units, mat, (((1,), (1,)), ((), ())), preferred_element_type=f32)
             result = result.astype(bf16)
-            lo = q * d_loc
-            ysend[b, :, lo : lo + d_loc] = result[cap:]
-            yb[b, 0:cap, lo : lo + d_loc] = result[:cap]
-        y_copy(b).start()
-    every(n_z, stage_f)
-
-    def rs_right(b):
-        return remote(rs_send.at[b], rs_recv.at[b], rs_sr.at[b], rs_r.at[b], fs=me + PAIR)
-
-    def rs_left(b):
+            ysend[b, q] = result[cap:]
+            y_copy(b, q).start()
+            yb[b, q, 0:cap, :] = result[:cap]
+    with jax.named_scope("every_n_z_stage_f_"):
+        every(n_z, stage_f)
+
+    def rs_right(b, q):
+        return remote(rs_send.at[b, q], rs_recv.at[b, q], rs_sr.at[b, q], rs_r.at[b, q], fs=me + PAIR)
+
+    def rs_left(b, q):
         at = jnp.where(b == z - 1, n_z, b)
-        return remote(rs_send.at[b], rs_recv.at[at], rs_sl.at[b], rs_r.at[at], fs=me - PAIR)
-
-    def rs_from(at):
-        return remote(rs_send.at[0], rs_recv.at[at], rs_sr.at[0], rs_r.at[at], fs=me)
+        return remote(rs_send.at[b, q], rs_recv.at[at, q], rs_sl.at[b, q], rs_r.at[at, q], fs=me - PAIR)
+
+    def rs_from(at, q):
+        return remote(rs_send.at[0, q], rs_recv.at[at, q], rs_sr.at[0, q], rs_r.at[at, q], fs=me)
 
     def stage_g(s):
         b = looked_up(far, z, s)
-        y_copy(b).wait_recv()
 
         def share(which):
             weights = jnp.broadcast_to(aux_recv[b, pl.ds(PAIR + which, 1), :], (cap, r_rows))
             return jnp.where(picker(b, which), weights, 0.0).astype(bf16)
         spreading = jnp.concatenate([share(x), share(1 - x)], axis=0)
-        acc[...] = lax.dot_general(spreading, yb[b], (((0,), (0,)), ((), ())), preferred_element_type=f32)
-
-        @pl.when(((b >= z) & (z > 0)) | ((b < z) & (z < n_z - 1)))
-        def _():
-            rs_from(b).wait_recv()
-            acc[...] += rs_recv[b].astype(f32)
-
-        @pl.when((b == z) & (z < n_z - 1))
-        def _():
-            rs_from(n_z).wait_recv()
-            acc[...] += rs_recv[n_z].astype(f32)
-
-        @pl.when(b != z)
-        def _():
-            rs_send[b] = acc[...].astype(bf16)
-
-        @pl.when(b > z)
-        def _():
-            rs_right(b).start()
-
-        @pl.when(b < z)
-        def _():
-            rs_left(b).start()
-
-        @pl.when(b == z)
-        def _():
-            mixed_out[...] = acc[...].astype(bf16)
-    every(n_z, stage_g)
+        for q in range(per_quarter):
+            y_copy(b, q).wait_recv()
+            acc[...] = lax.dot_general(spreading, yb[b, q], (((0,), (0,)), ((), ())), preferred_element_type=f32)
+
+            @pl.when(((b >= z) & (z > 0)) | ((b < z) & (z < n_z - 1)))
+            def _():
+                rs_from(b, q).wait_recv()
+                acc[...] += rs_recv[b, q].astype(f32)
+
+            @pl.when((b == z) & (z < n_z - 1))
+            def _():
+                rs_from(n_z, q).wait_recv()
+                acc[...] += rs_recv[n_z, q].astype(f32)
+
+            @pl.when(b != z)
+            def _():
+                rs_send[b, q] = acc[...].astype(bf16)
+
+            @pl.when(b > z)
+            def _():
+                rs_right(b, q).start()
+
+            @pl.when(b < z)
+            def _():
+                rs_left(b, q).start()
+
+            @pl.when(b == z)
+            def _():
+                mixed_out[:, q * d_loc : (q + 1) * d_loc] = acc[...].astype(bf16)
+    with jax.named_scope("every_n_z_stage_g_"):
+        every(n_z, stage_g)
 
     for d in range(1, n_tp):
         ssq_copy(d).wait_send()
@@ -557,23 +655,25 @@
     span(1, n_fs, sent_w)
 
     def sent_b(b):
-        @pl.when(goes_right(b))
+        @pl.when(goes_right(b) & ~(inner & (b == z - 2)))
         def _():
             ag_right(b).wait_send()
 
-        @pl.when(goes_left(b))
+        @pl.when(goes_left(b) & ~(inner & (b == z + 2)))
         def _():
             ag_left(b).wait_send()
-        for copy in (x_copy, rc_copy, ry_copy, rf_copy, hc_copy, hy_copy, hf_copy, y_copy):
+        for copy in (x_copy, rc_copy, ry_copy, rf_copy, hc_copy, hy_copy, hf_copy):
             copy(b).wait_send()
-
-        @pl.when(b > z)
-        def _():
-            rs_right(b).wait_send()
-
-        @pl.when(b < z)
-        def _():
-            rs_left(b).wait_send()
+        for q in range(per_quarter):
+            y_copy(b, q).wait_send()
+
+            @pl.when(b > z)
+            def _():
+                rs_right(b, q).wait_send()
+
+            @pl.when(b < z)
+            def _():
+                rs_left(b, q).wait_send()
     every(n_z, sent_b)
 
     def sent_j(j):
@@ -600,11 +700,11 @@
         ((n_z, cap, feat), bf16),
         ((n_tp, n_z, 2 * cap, h_cols), bf16),
         ((per_quarter, n_tp, d_loc, h_cols), bf16),
-        ((n_z, 2 * cap, feat), bf16),
-        ((n_z, cap, feat), bf16),
-        ((n_z, r_rows, feat), bf16),
-        ((n_z + 1, r_rows, feat), bf16),
-        ((r_rows, feat), f32),
+        ((n_z, per_quarter, 2 * cap, d_loc), bf16),
+        ((n_z, per_quarter, cap, d_loc), bf16),
+        ((n_z, per_quarter, r_rows, d_loc), bf16),
+        ((n_z + 1, per_quarter, r_rows, d_loc), bf16),
+        ((r_rows, d_loc), f32),
         ((n_tp, 8, r_rows), f32),
         ((n_z, 8, r_rows), f32),
         ((n_z, 8, r_rows), f32),
@@ -615,7 +715,8 @@
         (n_fs,), (n_fs,), (n_fs,), (n_fs,), (n_z,), (n_z,),
         (n_z,), (n_z,), (n_z,), (n_z,), (n_z,), (n_z,),
         (n_z,), (n_z,), (n_z,), (n_z,), (n_z,), (n_z,),
-        (n_fs,), (per_quarter, n_tp), (n_z,), (n_z,), (n_z,), (n_z,), (n_z + 1,), (3, n_fs),
+        (n_fs,), (per_quarter, n_tp), (n_z, per_quarter), (n_z, per_quarter),
+        (n_z, per_quarter), (n_z, per_quarter), (n_z + 1, per_quarter), (3, n_fs),
     ]
     return buffers, sems
 

time: 246 us -> 205 us (0.83)
  the two profiles are of different devices: /device:TPU:10 before, /device:TPU:5 now
where the time goes in v2:
time: 205 us; the launch traced here: 204 us
  Pallas kernels  198 us (97%)
  local copies, waits for them, and re-layouts  5.24 us (3%)
    pallas_call x1, Pallas kernels, body(): pl.pallas_call(functools.partial(moe_kernel, dims), out_shape=(matrix, ma...  198 us
    unnamed x10, local copies, waits for them, and re-layouts  5.24 us

profile of v2, /device:TPU:5, one launch (start us, length us, event | category | flops | bytes accessed | tf_op | source)
XLA Modules:
  0.0 204.0 jit_solution(13203683972098484747)
XLA Ops:
  0.6 198.1 %experts.1 = (bf16[4096,128]{1,0:T(8,128)(2,1)}, bf16[4096,128]{1,0:T(8,128)(2,1)}, bf16[4096,128]{1,0:T(8,128)(2,1)}, bf16[384,1024]{1,0:T(8,128)(2,1)}) custom-call(bf16[384,1024]{1,0:T(8,128)(2,1)} %tok.1, f32[1,512]{1,0:T(1,128)} %bitcast.11, s32[2,384]{1,0:T(2,128)} %bitcast.9, f32[2,384]{1,0:T(2,128)} %bitcast.10, f32[8,512,128]{2,1,0:T(8,128)} %gate_hbm.1, ...), custom_call_target="tpu_custom_call" | custom-call | tf_op jit(solution)/shard_map/experts/pallas_call | solution.py:755
  198.7 0.0 copy-start.1
  198.7 0.0 copy-start
  198.7 2.4 %copy.15 = bf16[1,4096,128]{2,1,0:T(8,128)(2,1)} copy(bf16[1,4096,128]{2,1,0:T(8,128)(2,1)} %bitcast.8) | data formatting | bytes 2097152
  201.1 0.0 copy-done.1
  201.1 0.0 copy-start.2
  201.1 1.0 copy.16
  202.1 0.0 copy-done
  202.1 1.0 copy.17
  203.1 0.0 copy-done.2
  203.1 0.9 copy.18
Async XLA Ops:
  198.7 2.4 %copy-start.1 = (bf16[4096,128]{1,0:T(8,128)(2,1)S(1)}, bf16[4096,128]{1,0:T(8,128)(2,1)}, u32[]{:S(2)}) copy-start(bf16[4096,128]{1,0:T(8,128)(2,1)} %get-tuple-element.9) | copy-start | bytes 3145732
  198.7 3.4 %copy-start = (bf16[4096,128]{1,0:T(8,128)(2,1)S(1)}, bf16[4096,128]{1,0:T(8,128)(2,1)}, u32[]{:S(2)}) copy-start(bf16[4096,128]{1,0:T(8,128)(2,1)} %get-tuple-element.10) | copy-start | bytes 3145732
  201.1 1.9 copy-start.2

commit v3 on v2

--- a/solution.py
+++ b/solution.py
@@ -162,7 +162,7 @@
 
 def far_first(n_z):
     def rank(z, b):
-        return (-abs(b - z), min(b, n_z - 1 - b), b)
+        return (-abs(b - z), -min(b, n_z - 1 - b), b)
 
     return [sorted(range(n_z), key=lambda b: rank(z, b)) for z in range(n_z)]
 
@@ -180,12 +180,13 @@
     tok, gain, routes, weight, gate_hbm, up_hbm, down_hbm,
     gate_out, up_out, down_out, mixed_out,
     stage, wgu_send, wd_send, wgu_recv, wd_recv, blk, rows, xsend, hid, dn, yb, ysend,
-    rs_send, rs_recv, acc, ssq, aux_send, aux_recv, gain_mat,
+    rs_send, rs_recv, acc, both, wd2, dn2, hid2, yb2, ysend2, ssq, aux_send, aux_recv, gain_mat,
     stage_sem, ssq_s, ssq_r, aux_s, aux_r, ag_sr, ag_sl, ag_r,
     wgu_s, wgu_r, wd_s, wd_r, x_s, x_r,
     rc_s, rc_r, ry_s, ry_r, rf_s, rf_r,
     hc_s, hc_r, hy_s, hy_r, hf_s, hf_r,
     dn_s, dn_r, y_s, y_r, rs_sr, rs_sl, rs_r, out_sem,
+    w2_s, w2_r, wf_s, d2_s, d2_r, h2_sem, y2_s, y2_r,
 ):
     n_fs, n_tp, n_z, r_rows, feat, d_loc, h_cols, cap = dims
     top_count = routes.shape[0]
@@ -271,6 +272,17 @@
         def _():
             ag_left(b).start()
     ag_start(z)
+
+    side = jnp.where(z < n_z // 2, 1, -1)
+    inner = (z > 0) & (z < n_z - 1)
+
+    def at(distance):
+        return z + side * distance
+
+    def help_copy(k):
+        src = wd_send.at[xp] if k == 0 else wd_recv.at[me]
+        column = 1 - x if k == 0 else x
+        return remote(src, wd2.at[me], w2_s.at[k], w2_r.at[me], fs=at(1) * PAIR + column)
 
     expert = lax.broadcasted_iota(jnp.int32, (n_fs, r_rows), 0)
     picks = [jnp.broadcast_to(routes[k : k + 1, :], (n_fs, r_rows)) == expert for k in range(top_count)]
@@ -297,7 +309,11 @@
         lo = plane * PAIR
         aux_send[plane, 0:PAIR, :] = slot_t[lo : lo + PAIR]
         aux_send[plane, PAIR : 2 * PAIR, :] = mixed_t[lo : lo + PAIR]
-        aux_send[plane, 2 * PAIR :, :] = inverse[2 * PAIR :]
+        aux_send[plane, 2 * PAIR : 8, :] = inverse[2 * PAIR :]
+        lo = 0 if plane < n_z // 2 else (n_z - 1) * PAIR
+        aux_send[plane, 8 : 8 + PAIR, :] = slot_t[lo : lo + PAIR]
+        aux_send[plane, 8 + PAIR : 8 + 2 * PAIR, :] = mixed_t[lo : lo + PAIR]
+        aux_send[plane, 8 + 2 * PAIR :, :] = inverse[2 * PAIR :]
     aux_recv[z] = aux_send[z]
 
     def aux_copy(d):
@@ -342,14 +358,25 @@
         wgu_copy(d).start()
 
     def send_d(d):
-        cast_d(d, wd_send, (me + d) % n_fs)
-        wd_copy(d).start()
+        e = (me + d) % n_fs
+        cast_d(d, wd_send, e)
+        plane = e // PAIR
+        helper = jnp.where(plane == 0, 1, n_z - 2) * PAIR + e % PAIR
+        by_helper = ((plane == 0) | (plane == n_z - 1)) & (plane != z) & (helper != me)
+
+        @pl.when(by_helper)
+        def _():
+            remote(wd_send.at[e], wd2.at[me], wd_s.at[d], w2_r.at[me], fs=helper).start()
+
+        @pl.when(~by_helper)
+        def _():
+            wd_copy(d).start()
 
     def span(first_d, last_d, body):
         every(last_d - first_d, lambda i: body(i + first_d))
 
-    def picker(b, which):
-        slots = aux_recv[b, pl.ds(which, 1), :]
+    def picker(b, which, base=0):
+        slots = aux_recv[b, pl.ds(base + which, 1), :]
         at = lax.broadcasted_iota(jnp.int32, (cap, r_rows), 0).astype(f32)
         return at == jnp.broadcast_to(slots, (cap, r_rows))
 
@@ -395,33 +422,9 @@
         ry_copy(b).wait_recv()
         rf_copy(b).start()
 
-    def plane_sends(plane, body):
-        for k in range(PAIR):
-            body((plane * PAIR + k + n_fs - me) % n_fs)
-
-    def side_sends(to_right, body):
-        for d in range(1, n_z):
-            if to_right:
-                @pl.when(z + d < n_z)
-                def _():
-                    plane_sends(z + d, body)
-            else:
-                @pl.when(z >= d)
-                def _():
-                    plane_sends(z - d, body)
-
-    def shorter_side(body):
-        right = z < n_z // 2
-
-        @pl.when(right)
-        def _():
-            side_sends(False, body)
-
-        @pl.when(~right)
-        def _():
-            side_sends(True, body)
-
-    inner = (z > 0) & (z < n_z - 1)
+    def plane_send(plane, column, body):
+        body((plane * PAIR + column + n_fs - me) % n_fs)
+
 
     def partner_sends(body):
         body((xp + n_fs - me) % n_fs)
@@ -429,6 +432,84 @@
     def named(kind, s):
         with jax.named_scope(kind + str(s)):
             {"a": stage_a, "b": stage_b, "c": stage_c}[kind](s)
+
+    def out_copies(j):
+        at = pl.ds(pl.multiple_of(j * d_loc, d_loc), d_loc)
+        return [
+            pltpu.make_async_copy(wgu_recv.at[j, :, pl.ds(0, h_cols)], gate_out.at[at], out_sem.at[0, j]),
+            pltpu.make_async_copy(wgu_recv.at[j, :, pl.ds(h_cols, h_cols)], up_out.at[at], out_sem.at[1, j]),
+            pltpu.make_async_copy(wd_recv.at[j], down_out.at[at], out_sem.at[2, j]),
+        ]
+
+    def dn_copy(j):
+        q = j % per_quarter
+        return remote(wd_recv.at[j], dn.at[q, t], dn_s.at[j], dn_r.at[q, t], tp=j // per_quarter)
+
+    def dn_from(q, k):
+        return remote(wd_recv.at[0], dn.at[q, k], dn_s.at[0], dn_r.at[q, k], tp=t)
+
+    def pass_down(j):
+        @pl.when(j != me)
+        def _():
+            wd_from(j).wait_recv()
+
+        @pl.when(j // per_quarter == t)
+        def _():
+            dn[j % per_quarter, t] = wd_recv[j]
+
+        @pl.when(j // per_quarter != t)
+        def _():
+            dn_copy(j).start()
+        out_copies(j)[2].start()
+
+    def pass_plane(s):
+        plane = looked_up(near, z, s)
+        for k in range(PAIR):
+            pass_down(plane * PAIR + k)
+
+    def wf_copy(j):
+        return remote(wd2.at[j], wd_recv.at[j], wf_s.at[j], wd_r.at[j], fs=at(-1) * PAIR + x)
+
+    def d2_copy(j):
+        q = j % per_quarter
+        return remote(wd2.at[j], dn2.at[q, t], d2_s.at[j], d2_r.at[q, t], tp=j // per_quarter)
+
+    def pass_for_end(j):
+        @pl.when(j == me)
+        def _():
+            wd2[j] = wd_send[at(-1) * PAIR + x]
+
+        @pl.when(j != me)
+        def _():
+            wd_copy_at = remote(wd2.at[j], wd2.at[j], w2_s.at[0], w2_r.at[j], fs=me)
+            wd_copy_at.wait_recv()
+
+        @pl.when((j != me) & (j // PAIR != at(-1)))
+        def _():
+            wf_copy(j).start()
+
+    def pass_end(j):
+        @pl.when(j // per_quarter == t)
+        def _():
+            dn2[j % per_quarter, t] = wd2[j]
+
+        @pl.when(j // per_quarter != t)
+        def _():
+            d2_copy(j).start()
+
+    def help_end():
+        for distance in (0, -1, 1, 2):
+            for k in range(PAIR):
+                pass_for_end(at(distance) * PAIR + k)
+
+    def own_weights():
+        cast_gu(0, wgu_recv, me)
+        cast_d(0, wd_recv, me)
+
+    def outer_own():
+        own_weights()
+        for k in range(PAIR):
+            help_copy(k).start()
 
     def run(*steps):
         for step in steps:
@@ -438,14 +519,16 @@
                 with jax.named_scope("w"):
                     step()
 
-    def toward(distance, body):
+    def toward(distance, column, *bodies):
         @pl.when(z < n_z // 2)
         def _():
-            plane_sends(z + distance, body)
+            for each in bodies:
+                plane_send(z + distance, column, each)
 
         @pl.when(z >= n_z // 2)
         def _():
-            plane_sends(z - distance, body)
+            for each in bodies:
+                plane_send(z - distance, column, each)
 
     def forwarded():
         @pl.when(z < n_z // 2)
@@ -460,42 +543,34 @@
         partner_sends(send_gu)
         partner_sends(send_d)
 
-    def inner_second():
-        forwarded()
-        toward(2, send_gu)
-        shorter_side(send_gu)
-
-    def inner_third():
-        toward(1, send_d)
-        toward(2, send_d)
-        shorter_side(send_d)
-
-    def outer_first():
-        toward(1, send_gu)
-        toward(1, send_d)
-
-    def outer_third():
-        toward(2, send_d)
-        toward(3, send_d)
+    def inner_second(body):
+        toward(-1, x, body)
+        toward(1, 1 - x, body)
+        toward(-1, 1 - x, body)
 
     @pl.when(inner)
     def _():
-        run("a0", partner_all, "b0", "a1", "a2", "b1", "c0", "a3", lambda: toward(1, send_gu),
-            "b2", "c1", inner_second, "b3", "c2", inner_third)
+        run("a0", partner_all, "b0", "a1", "a2", "c0", "a3",
+            lambda: toward(2, x, send_d), lambda: toward(2, 1 - x, send_d), lambda: toward(1, x, send_gu, send_d),
+            "b1", "b2", forwarded, lambda: inner_second(send_d), "c1", "b3",
+            lambda: toward(2, x, send_gu), lambda: inner_second(send_gu), lambda: toward(2, 1 - x, send_gu),
+            own_weights, help_end, "c2")
+
+    def outer_second(body):
+        for distance in range(1, n_z - 1):
+            toward(distance, 1 - x, body)
 
     @pl.when(~inner)
     def _():
-        run("a0", partner_all, "b0", "a1", outer_first, "b1", "c0", "a2", lambda: toward(2, send_gu),
-            "b2", "c1", "a3", lambda: toward(3, send_gu), "b3", "c2", outer_third)
-    cast_gu(0, wgu_recv, me)
-    cast_d(0, wd_recv, me)
+        run("a0", partner_all, "b0", "a1", lambda: toward(1, x, send_gu, send_d), "b1", "c0", outer_own,
+            "a2", lambda: toward(3, x, send_d), lambda: toward(3, 1 - x, send_d),
+            lambda: toward(2, x, send_gu, send_d), "b2", "c1", "a3", lambda: outer_second(send_d), "b3",
+            lambda: toward(3, x, send_gu), lambda: outer_second(send_gu), lambda: toward(3, 1 - x, send_gu), "c2")
+    with jax.named_scope("pass_own"):
+        pass_plane(0)
     with jax.named_scope("c3"):
         stage_c(3)
 
-    def wait_gu(d):
-        wgu_from((me + n_fs - d) % n_fs).wait_recv()
-    with jax.named_scope("span_1_n_fs_wait_gu_"):
-        span(1, n_fs, wait_gu)
 
     def hc_copy(b):
         return remote(hid.at[t, b], hid.at[t, b], hc_s.at[b], hc_r.at[b], tp=tc)
@@ -506,69 +581,73 @@
     def hf_copy(b):
         return remote(hid.at[ty, b], hid.at[ty, b], hf_s.at[b], hf_r.at[b], tp=tc)
 
-    def stage_d(s):
-        b = looked_up(far, z, s)
+    def h2_copy(b):
+        return remote(hid.at[t, b], hid2.at[t], h2_sem.at[0], h2_sem.at[1], fs=at(1) * PAIR + x)
+
+    def h2y_copy():
+        return remote(hid2.at[t], hid2.at[t], h2_sem.at[2], h2_sem.at[3], tp=ty)
+
+    def h2c_copy():
+        return remote(hid2.at[t], hid2.at[t], h2_sem.at[4], h2_sem.at[5], tp=tc)
+
+    def h2f_copy():
+        return remote(hid2.at[ty], hid2.at[ty], h2_sem.at[6], h2_sem.at[7], tp=tc)
+
+    def rows_ready(b):
         rc_copy(b).wait_recv()
         rf_copy(b).wait_recv()
-        both = jnp.zeros((2 * cap, 2 * h_cols), f32)
-        for j in range(n_fs):
-            lo = (j % per_quarter) * d_loc
-            both = both + jnp.dot(rows[j // per_quarter, b, :, lo : lo + d_loc], wgu_recv[j],
-                                  preferred_element_type=f32)
-        gates = both[:, 0:h_cols]
-        hid[t, b] = (gates / (1.0 + jnp.exp(-gates)) * both[:, h_cols:]).astype(bf16)
-        hy_copy(b).start()
-        hc_copy(b).start()
-    with jax.named_scope("every_n_z_stage_d_"):
-        every(n_z, stage_d)
-
-    def out_copies(j):
-        at = pl.ds(pl.multiple_of(j * d_loc, d_loc), d_loc)
-        return [
-            pltpu.make_async_copy(wgu_recv.at[j, :, pl.ds(0, h_cols)], gate_out.at[at], out_sem.at[0, j]),
-            pltpu.make_async_copy(wgu_recv.at[j, :, pl.ds(h_cols, h_cols)], up_out.at[at], out_sem.at[1, j]),
-            pltpu.make_async_copy(wd_recv.at[j], down_out.at[at], out_sem.at[2, j]),
-        ]
-
-    def dn_copy(j):
-        q = j % per_quarter
-        return remote(wd_recv.at[j], dn.at[q, t], dn_s.at[j], dn_r.at[q, t], tp=j // per_quarter)
-
-    def dn_from(q, k):
-        return remote(wd_recv.at[0], dn.at[q, k], dn_s.at[0], dn_r.at[q, k], tp=t)
-
-    def pass_down(j):
-        @pl.when(j != me)
-        def _():
-            wd_from(j).wait_recv()
-
-        @pl.when(j // per_quarter == t)
-        def _():
-            dn[j % per_quarter, t] = wd_recv[j]
-
-        @pl.when(j // per_quarter != t)
-        def _():
-            dn_copy(j).start()
-        for copy in out_copies(j):
-            copy.start()
-
-    def pass_planes(first_s, last_s):
-        def one(s):
-            plane = looked_up(near, z, s)
-            for k in range(PAIR):
-                pass_down(plane * PAIR + k)
-        span(first_s, last_s, one)
-    with jax.named_scope("pass_near"):
-        pass_planes(0, n_z // 2)
+
+    def add_piece(j):
+        lo = pl.ds(pl.multiple_of((j % per_quarter) * d_loc, d_loc), d_loc)
+
+        def one(b):
+            both[b] += jnp.dot(rows[j // per_quarter, b, :, lo], wgu_recv[j], preferred_element_type=f32)
+        every(n_z, one)
+
+    def add_plane(s):
+        plane = looked_up(near, z, s)
+        for k in range(PAIR):
+            j = plane * PAIR + k
+
+            @pl.when(j != me)
+            def _():
+                wgu_from(j).wait_recv()
+            for copy in out_copies(j)[:2]:
+                copy.start()
+            add_piece(j)
+
+    def stage_h(s):
+        b = looked_up(far, z, s)
+        gates = both[b, :, 0:h_cols]
+        hid[t, b] = (gates / (1.0 + jnp.exp(-gates)) * both[b, :, h_cols:]).astype(bf16)
+        apart = ~inner & (b == at(3))
+
+        @pl.when(apart)
+        def _():
+            h2_copy(b).start()
+
+        @pl.when(~apart)
+        def _():
+            hy_copy(b).start()
+            hc_copy(b).start()
+    both[...] = jnp.zeros(both.shape, f32)
+    with jax.named_scope("pass"):
+        span(1, n_z, pass_plane)
+
+    @pl.when(inner)
+    def _():
+        every(n_fs, pass_end)
+    with jax.named_scope("rows"):
+        every(n_z, rows_ready)
+    with jax.named_scope("gu"):
+        every(n_z, add_plane)
+    with jax.named_scope("h"):
+        every(n_z, stage_h)
 
     def stage_e(s):
         b = looked_up(far, z, s)
         hy_copy(b).wait_recv()
         hf_copy(b).start()
-    with jax.named_scope("every_n_z_stage_e_"):
-        every(n_z, stage_e)
-    with jax.named_scope("pass_far"):
-        pass_planes(n_z // 2, n_z)
 
     def wait_dn(d):
         k = (t + d) % n_tp
@@ -592,8 +671,37 @@
             ysend[b, q] = result[cap:]
             y_copy(b, q).start()
             yb[b, q, 0:cap, :] = result[:cap]
-    with jax.named_scope("every_n_z_stage_f_"):
-        every(n_z, stage_f)
+    def y2_copy(q):
+        return remote(ysend2.at[q], yb2.at[q, pl.ds(cap, cap)], y2_s.at[q], y2_r.at[q], fs=xp)
+
+    def result_of(s):
+        stage_e(s)
+        stage_f(s)
+
+    def end_hidden():
+        h2_copy(at(2)).wait_recv()
+        h2y_copy().start()
+        h2c_copy().start()
+        h2y_copy().wait_recv()
+        h2f_copy().start()
+
+    def wait_dn2(d):
+        k = (t + d) % n_tp
+        for q in range(per_quarter):
+            remote(wd2.at[0], dn2.at[q, k], d2_s.at[0], d2_r.at[q, k], tp=t).wait_recv()
+
+    def end_results():
+        span(1, n_tp, wait_dn2)
+        h2c_copy().wait_recv()
+        h2f_copy().wait_recv()
+        units = jnp.concatenate([hid2[k] for k in range(n_tp)], axis=1)
+        for q in range(per_quarter):
+            mat = jnp.concatenate([dn2[q, k] for k in range(n_tp)], axis=1)
+            result = lax.dot_general(units, mat, (((1,), (1,)), ((), ())), preferred_element_type=f32)
+            result = result.astype(bf16)
+            ysend2[q] = result[cap:]
+            y2_copy(q).start()
+            yb2[q, 0:cap, :] = result[:cap]
 
     def rs_right(b, q):
         return remote(rs_send.at[b, q], rs_recv.at[b, q], rs_sr.at[b, q], rs_r.at[b, q], fs=me + PAIR)
@@ -605,44 +713,71 @@
     def rs_from(at, q):
         return remote(rs_send.at[0, q], rs_recv.at[at, q], rs_sr.at[0, q], rs_r.at[at, q], fs=me)
 
-    def stage_g(s):
+    def stage_g(s, q):
         b = looked_up(far, z, s)
 
-        def share(which):
-            weights = jnp.broadcast_to(aux_recv[b, pl.ds(PAIR + which, 1), :], (cap, r_rows))
-            return jnp.where(picker(b, which), weights, 0.0).astype(bf16)
+        helped = inner & (b == at(2))
+
+        def share(which, base=0):
+            weights = jnp.broadcast_to(aux_recv[b, pl.ds(base + PAIR + which, 1), :], (cap, r_rows))
+            return jnp.where(picker(b, which, base), weights, 0.0).astype(bf16)
         spreading = jnp.concatenate([share(x), share(1 - x)], axis=0)
-        for q in range(per_quarter):
-            y_copy(b, q).wait_recv()
-            acc[...] = lax.dot_general(spreading, yb[b, q], (((0,), (0,)), ((), ())), preferred_element_type=f32)
-
-            @pl.when(((b >= z) & (z > 0)) | ((b < z) & (z < n_z - 1)))
-            def _():
-                rs_from(b, q).wait_recv()
-                acc[...] += rs_recv[b, q].astype(f32)
-
-            @pl.when((b == z) & (z < n_z - 1))
-            def _():
-                rs_from(n_z, q).wait_recv()
-                acc[...] += rs_recv[n_z, q].astype(f32)
-
-            @pl.when(b != z)
-            def _():
-                rs_send[b, q] = acc[...].astype(bf16)
-
-            @pl.when(b > z)
-            def _():
-                rs_right(b, q).start()
-
-            @pl.when(b < z)
-            def _():
-                rs_left(b, q).start()
-
-            @pl.when(b == z)
-            def _():
-                mixed_out[:, q * d_loc : (q + 1) * d_loc] = acc[...].astype(bf16)
-    with jax.named_scope("every_n_z_stage_g_"):
-        every(n_z, stage_g)
+        y_copy(b, q).wait_recv()
+        acc[...] = lax.dot_general(spreading, yb[b, q], (((0,), (0,)), ((), ())), preferred_element_type=f32)
+
+        @pl.when(helped)
+        def _():
+            y2_copy(q).wait_recv()
+            more = jnp.concatenate([share(x, 8), share(1 - x, 8)], axis=0)
+            acc[...] += lax.dot_general(more, yb2[q], (((0,), (0,)), ((), ())), preferred_element_type=f32)
+
+        @pl.when((((b >= z) & (z > 0)) | ((b < z) & (z < n_z - 1))) & ~helped)
+        def _():
+            rs_from(b, q).wait_recv()
+            acc[...] += rs_recv[b, q].astype(f32)
+
+        @pl.when((b == z) & (z < n_z - 1))
+        def _():
+            rs_from(n_z, q).wait_recv()
+            acc[...] += rs_recv[n_z, q].astype(f32)
+
+        @pl.when(b != z)
+        def _():
+            rs_send[b, q] = acc[...].astype(bf16)
+
+        @pl.when(b > z)
+        def _():
+            rs_right(b, q).start()
+
+        @pl.when(b < z)
+        def _():
+            rs_left(b, q).start()
+
+        @pl.when(b == z)
+        def _():
+            mixed_out[:, q * d_loc : (q + 1) * d_loc] = acc[...].astype(bf16)
+    def in_turn(*steps):
+        for name, step, *given in steps:
+            with jax.named_scope(name):
+                step(*given)
+
+    @pl.when(inner)
+    def _():
+        in_turn(
+            ("f0", result_of, 0), ("e2", end_hidden), ("f2", end_results),
+            ("g00", stage_g, 0, 0), ("f1", result_of, 1), ("g01", stage_g, 0, 1),
+            ("g10", stage_g, 1, 0), ("f2", result_of, 2), ("g11", stage_g, 1, 1),
+            ("f3", result_of, 3), ("g20", stage_g, 2, 0), ("g21", stage_g, 2, 1),
+            ("g30", stage_g, 3, 0), ("g31", stage_g, 3, 1),
+        )
+
+    @pl.when(~inner)
+    def _():
+        in_turn(
+            ("f1", result_of, 1), ("g10", stage_g, 1, 0), ("f2", result_of, 2), ("g11", stage_g, 1, 1),
+            ("g20", stage_g, 2, 0), ("f3", result_of, 3), ("g21", stage_g, 2, 1),
+            ("g30", stage_g, 3, 0), ("g31", stage_g, 3, 1),
+        )
 
     for d in range(1, n_tp):
         ssq_copy(d).wait_send()
@@ -662,21 +797,54 @@
         @pl.when(goes_left(b) & ~(inner & (b == z + 2)))
         def _():
             ag_left(b).wait_send()
-        for copy in (x_copy, rc_copy, ry_copy, rf_copy, hc_copy, hy_copy, hf_copy):
+        for copy in (x_copy, rc_copy, ry_copy, rf_copy):
             copy(b).wait_send()
-        for q in range(per_quarter):
-            y_copy(b, q).wait_send()
-
-            @pl.when(b > z)
-            def _():
+        apart = ~inner & (b == at(3))
+
+        @pl.when(apart)
+        def _():
+            h2_copy(b).wait_send()
+
+        @pl.when(~apart)
+        def _():
+            for copy in (hc_copy, hy_copy, hf_copy):
+                copy(b).wait_send()
+            for q in range(per_quarter):
+                y_copy(b, q).wait_send()
+
+        @pl.when((b > z) & ~apart)
+        def _():
+            for q in range(per_quarter):
                 rs_right(b, q).wait_send()
 
-            @pl.when(b < z)
-            def _():
+        @pl.when((b < z) & ~apart)
+        def _():
+            for q in range(per_quarter):
                 rs_left(b, q).wait_send()
     every(n_z, sent_b)
 
+    @pl.when(inner)
+    def _():
+        h2y_copy().wait_send()
+        h2c_copy().wait_send()
+        h2f_copy().wait_send()
+        for q in range(per_quarter):
+            y2_copy(q).wait_send()
+
+    @pl.when(~inner)
+    def _():
+        for k in range(PAIR):
+            help_copy(k).wait_send()
+
     def sent_j(j):
+        @pl.when(inner & (j != me) & (j // PAIR != at(-1)))
+        def _():
+            wf_copy(j).wait_send()
+
+        @pl.when(inner & (j // per_quarter != t))
+        def _():
+            d2_copy(j).wait_send()
+
         @pl.when(j // per_quarter != t)
         def _():
             dn_copy(j).wait_send()
@@ -705,9 +873,15 @@
         ((n_z, per_quarter, r_rows, d_loc), bf16),
         ((n_z + 1, per_quarter, r_rows, d_loc), bf16),
         ((r_rows, d_loc), f32),
+        ((n_z, 2 * cap, 2 * h_cols), f32),
+        ((n_fs, d_loc, h_cols), bf16),
+        ((per_quarter, n_tp, d_loc, h_cols), bf16),
+        ((n_tp, 2 * cap, h_cols), bf16),
+        ((per_quarter, 2 * cap, d_loc), bf16),
+        ((per_quarter, cap, d_loc), bf16),
         ((n_tp, 8, r_rows), f32),
-        ((n_z, 8, r_rows), f32),
-        ((n_z, 8, r_rows), f32),
+        ((n_z, 16, r_rows), f32),
+        ((n_z, 16, r_rows), f32),
         ((d_loc, h_cols), f32),
     ]
     sems = [
@@ -717,6 +891,7 @@
         (n_z,), (n_z,), (n_z,), (n_z,), (n_z,), (n_z,),
         (n_fs,), (per_quarter, n_tp), (n_z, per_quarter), (n_z, per_quarter),
         (n_z, per_quarter), (n_z, per_quarter), (n_z + 1, per_quarter), (3, n_fs),
+        (PAIR,), (n_fs,), (n_fs,), (n_fs,), (per_quarter, n_tp), (8,), (per_quarter,), (per_quarter,),
     ]
     return buffers, sems
 

time: 205 us -> 185 us (0.902)
  Pallas kernels: 198 us -> 179 us
    pallas_call x1, Pallas kernels: 198 us -> 179 us  [body(): pl.pallas_call(functools.partial(moe_kernel, dims), out_shape=(matrix, ma...]
where the time goes in v3:
time: 185 us
  Pallas kernels  179 us (97%)
  local copies, waits for them, and re-layouts  5.24 us (3%)
    pallas_call x1, Pallas kernels, body(): pl.pallas_call(functools.partial(moe_kernel, dims), out_shape=(matrix, ma...  179 us
    unnamed x10, local copies, waits for them, and re-layouts  5.24 us

profile of v3, /device:TPU:5, one launch (start us, length us, event | category | flops | bytes accessed | tf_op | source)
XLA Modules:
  0.0 185.2 jit_solution(17191484591777615701)
XLA Ops:
  0.6 179.3 %experts.1 = (bf16[4096,128]{1,0:T(8,128)(2,1)}, bf16[4096,128]{1,0:T(8,128)(2,1)}, bf16[4096,128]{1,0:T(8,128)(2,1)}, bf16[384,1024]{1,0:T(8,128)(2,1)}) custom-call(bf16[384,1024]{1,0:T(8,128)(2,1)} %tok.1, f32[1,512]{1,0:T(1,128)} %bitcast.11, s32[2,384]{1,0:T(2,128)} %bitcast.9, f32[2,384]{1,0:T(2,128)} %bitcast.10, f32[8,512,128]{2,1,0:T(8,128)} %gate_hbm.1, ...), custom_call_target="tpu_custom_call" | custom-call | tf_op jit(solution)/shard_map/experts/pallas_call | solution.py:930
  179.9 0.0 copy-start.1
  179.9 0.0 copy-start
  180.0 2.4 %copy.15 = bf16[1,4096,128]{2,1,0:T(8,128)(2,1)} copy(bf16[1,4096,128]{2,1,0:T(8,128)(2,1)} %bitcast.8) | data formatting | bytes 2097152
  182.4 0.0 copy-done.1
  182.4 0.0 copy-start.2
  182.4 1.0 copy.16
  183.3 0.0 copy-done
  183.3 1.0 copy.17
  184.3 0.0 copy-done.2
  184.3 0.9 copy.18
Async XLA Ops:
  179.9 2.4 %copy-start.1 = (bf16[4096,128]{1,0:T(8,128)(2,1)S(1)}, bf16[4096,128]{1,0:T(8,128)(2,1)}, u32[]{:S(2)}) copy-start(bf16[4096,128]{1,0:T(8,128)(2,1)} %get-tuple-element.9) | copy-start | bytes 3145732
  179.9 3.4 %copy-start = (bf16[4096,128]{1,0:T(8,128)(2,1)S(1)}, bf16[4096,128]{1,0:T(8,128)(2,1)}, u32[]{:S(2)}) copy-start(bf16[4096,128]{1,0:T(8,128)(2,1)} %get-tuple-element.10) | copy-start | bytes 3145732
  182.4 1.9 %copy-start.2 = (bf16[384,1024]{1,0:T(8,128)(2,1)S(1)}, bf16[384,1024]{1,0:T(8,128)(2,1)}, u32[]{:S(2)}) copy-start(bf16[384,1024]{1,0:T(8,128)(2,1)} %get-tuple-element.19) | copy-start | bytes 2359300

commit v4 on v3

--- a/solution.py
+++ b/solution.py
@@ -186,7 +186,7 @@
     rc_s, rc_r, ry_s, ry_r, rf_s, rf_r,
     hc_s, hc_r, hy_s, hy_r, hf_s, hf_r,
     dn_s, dn_r, y_s, y_r, rs_sr, rs_sl, rs_r, out_sem,
-    w2_s, w2_r, wf_s, d2_s, d2_r, h2_sem, y2_s, y2_r,
+    w2_s, w2_r, wf_s, d2_s, d2_r, h2_sem, y2_s, y2_r, mixed_sem,
 ):
     n_fs, n_tp, n_z, r_rows, feat, d_loc, h_cols, cap = dims
     top_count = routes.shape[0]
@@ -383,6 +383,10 @@
     def x_copy(b):
         return remote(xsend.at[b], rows.at[t, b, pl.ds(cap, cap)], x_s.at[b], x_r.at[b], fs=xp)
 
+    def ry_copy(b, part):
+        some = rows.at[t, b, pl.ds(part * cap, cap)]
+        return remote(some, some, ry_s.at[b, part], ry_r.at[b, part], tp=ty)
+
     def stage_a(s):
         b = looked_up(near, z, s)
 
@@ -401,12 +405,11 @@
         xsend[b] = compact(1 - x)
         x_copy(b).start()
         rows[t, b, 0:cap, :] = compact(x)
+        ry_copy(b, 0).start()
 
     def rc_copy(b):
         return remote(rows.at[t, b], rows.at[t, b], rc_s.at[b], rc_r.at[b], tp=tc)
 
-    def ry_copy(b):
-        return remote(rows.at[t, b], rows.at[t, b], ry_s.at[b], ry_r.at[b], tp=ty)
 
     def rf_copy(b):
         return remote(rows.at[ty, b], rows.at[ty, b], rf_s.at[b], rf_r.at[b], tp=tc)
@@ -414,12 +417,13 @@
     def stage_b(s):
         b = looked_up(near, z, s)
         x_copy(b).wait_recv()
-        ry_copy(b).start()
+        ry_copy(b, 1).start()
         rc_copy(b).start()
 
     def stage_c(s):
         b = looked_up(near, z, s)
-        ry_copy(b).wait_recv()
+        for part in range(2):
+            ry_copy(b, part).wait_recv()
         rf_copy(b).start()
 
     def plane_send(plane, column, body):
@@ -433,13 +437,12 @@
         with jax.named_scope(kind + str(s)):
             {"a": stage_a, "b": stage_b, "c": stage_c}[kind](s)
 
-    def out_copies(j):
-        at = pl.ds(pl.multiple_of(j * d_loc, d_loc), d_loc)
-        return [
-            pltpu.make_async_copy(wgu_recv.at[j, :, pl.ds(0, h_cols)], gate_out.at[at], out_sem.at[0, j]),
-            pltpu.make_async_copy(wgu_recv.at[j, :, pl.ds(h_cols, h_cols)], up_out.at[at], out_sem.at[1, j]),
-            pltpu.make_async_copy(wd_recv.at[j], down_out.at[at], out_sem.at[2, j]),
-        ]
+    def out_copy(j, i):
+        to = pl.ds(pl.multiple_of(j * d_loc, d_loc), d_loc)
+        if i == 2:
+            return pltpu.make_async_copy(wd_recv.at[j], down_out.at[to], out_sem.at[2, j])
+        piece = wgu_recv.at[j, :, pl.ds(i * h_cols, h_cols)]
+        return pltpu.make_async_copy(piece, (gate_out, up_out)[i].at[to], out_sem.at[i, j])
 
     def dn_copy(j):
         q = j % per_quarter
@@ -460,7 +463,7 @@
         @pl.when(j // per_quarter != t)
         def _():
             dn_copy(j).start()
-        out_copies(j)[2].start()
+        out_copy(j, 2).start()
 
     def pass_plane(s):
         plane = looked_up(near, z, s)
@@ -612,8 +615,8 @@
             @pl.when(j != me)
             def _():
                 wgu_from(j).wait_recv()
-            for copy in out_copies(j)[:2]:
-                copy.start()
+            for i in range(2):
+                out_copy(j, i).start()
             add_piece(j)
 
     def stage_h(s):
@@ -641,9 +644,6 @@
         every(n_z, rows_ready)
     with jax.named_scope("gu"):
         every(n_z, add_plane)
-    with jax.named_scope("h"):
-        every(n_z, stage_h)
-
     def stage_e(s):
         b = looked_up(far, z, s)
         hy_copy(b).wait_recv()
@@ -659,24 +659,22 @@
     def y_copy(b, q):
         return remote(ysend.at[b, q], yb.at[b, q, pl.ds(cap, cap)], y_s.at[b, q], y_r.at[b, q], fs=xp)
 
-    def stage_f(s):
+    def stage_f(s, q):
         b = looked_up(far, z, s)
-        hc_copy(b).wait_recv()
-        hf_copy(b).wait_recv()
+        if q == 0:
+            stage_e(s)
+            hc_copy(b).wait_recv()
+            hf_copy(b).wait_recv()
         units = jnp.concatenate([hid[k, b] for k in range(n_tp)], axis=1)
-        for q in range(per_quarter):
-            mat = jnp.concatenate([dn[q, k] for k in range(n_tp)], axis=1)
-            result = lax.dot_general(units, mat, (((1,), (1,)), ((), ())), preferred_element_type=f32)
-            result = result.astype(bf16)
-            ysend[b, q] = result[cap:]
-            y_copy(b, q).start()
-            yb[b, q, 0:cap, :] = result[:cap]
+        mat = jnp.concatenate([dn[q, k] for k in range(n_tp)], axis=1)
+        result = lax.dot_general(units, mat, (((1,), (1,)), ((), ())), preferred_element_type=f32)
+        result = result.astype(bf16)
+        ysend[b, q] = result[cap:]
+        y_copy(b, q).start()
+        yb[b, q, 0:cap, :] = result[:cap]
+
     def y2_copy(q):
         return remote(ysend2.at[q], yb2.at[q, pl.ds(cap, cap)], y2_s.at[q], y2_r.at[q], fs=xp)
-
-    def result_of(s):
-        stage_e(s)
-        stage_f(s)
 
     def end_hidden():
         h2_copy(at(2)).wait_recv()
@@ -690,18 +688,18 @@
         for q in range(per_quarter):
             remote(wd2.at[0], dn2.at[q, k], d2_s.at[0], d2_r.at[q, k], tp=t).wait_recv()
 
-    def end_results():
-        span(1, n_tp, wait_dn2)
-        h2c_copy().wait_recv()
-        h2f_copy().wait_recv()
+    def end_results(q):
+        if q == 0:
+            span(1, n_tp, wait_dn2)
+            h2c_copy().wait_recv()
+            h2f_copy().wait_recv()
         units = jnp.concatenate([hid2[k] for k in range(n_tp)], axis=1)
-        for q in range(per_quarter):
-            mat = jnp.concatenate([dn2[q, k] for k in range(n_tp)], axis=1)
-            result = lax.dot_general(units, mat, (((1,), (1,)), ((), ())), preferred_element_type=f32)
-            result = result.astype(bf16)
-            ysend2[q] = result[cap:]
-            y2_copy(q).start()
-            yb2[q, 0:cap, :] = result[:cap]
+        mat = jnp.concatenate([dn2[q, k] for k in range(n_tp)], axis=1)
+        result = lax.dot_general(units, mat, (((1,), (1,)), ((), ())), preferred_element_type=f32)
+        result = result.astype(bf16)
+        ysend2[q] = result[cap:]
+        y2_copy(q).start()
+        yb2[q, 0:cap, :] = result[:cap]
 
     def rs_right(b, q):
         return remote(rs_send.at[b, q], rs_recv.at[b, q], rs_sr.at[b, q], rs_r.at[b, q], fs=me + PAIR)
@@ -712,6 +710,10 @@
 
     def rs_from(at, q):
         return remote(rs_send.at[0, q], rs_recv.at[at, q], rs_sr.at[0, q], rs_r.at[at, q], fs=me)
+
+    def mixed_copy(q):
+        lanes = pl.ds(q * d_loc, d_loc)
+        return pltpu.make_async_copy(rs_send.at[z, q], mixed_out.at[:, lanes], mixed_sem.at[q])
 
     def stage_g(s, q):
         b = looked_up(far, z, s)
@@ -755,7 +757,70 @@
 
         @pl.when(b == z)
         def _():
-            mixed_out[:, q * d_loc : (q + 1) * d_loc] = acc[...].astype(bf16)
+            rs_send[b, q] = acc[...].astype(bf16)
+            mixed_copy(q).start()
+    def settle():
+        for d in range(1, n_tp):
+            ssq_copy(d).wait_send()
+        for d in range(1, n_z):
+            aux_copy(d).wait_send()
+
+        def sent_w(d):
+            wgu_copy(d).wait_send()
+            wd_copy(d).wait_send()
+        span(1, n_fs, sent_w)
+
+        def sent_b(b):
+            @pl.when(goes_right(b) & ~(inner & (b == z - 2)))
+            def _():
+                ag_right(b).wait_send()
+
+            @pl.when(goes_left(b) & ~(inner & (b == z + 2)))
+            def _():
+                ag_left(b).wait_send()
+            for copy in (x_copy, rc_copy, rf_copy):
+                copy(b).wait_send()
+            for part in range(2):
+                ry_copy(b, part).wait_send()
+            apart = ~inner & (b == at(3))
+
+            @pl.when(apart)
+            def _():
+                h2_copy(b).wait_send()
+
+            @pl.when(~apart)
+            def _():
+                for copy in (hc_copy, hy_copy, hf_copy):
+                    copy(b).wait_send()
+        every(n_z, sent_b)
+
+        @pl.when(inner)
+        def _():
+            h2y_copy().wait_send()
+            h2c_copy().wait_send()
+            h2f_copy().wait_send()
+
+        @pl.when(~inner)
+        def _():
+            for k in range(PAIR):
+                help_copy(k).wait_send()
+
+        def sent_j(j):
+            @pl.when(inner & (j != me) & (j // PAIR != at(-1)))
+            def _():
+                wf_copy(j).wait_send()
+
+            @pl.when(inner & (j // per_quarter != t))
+            def _():
+                d2_copy(j).wait_send()
+
+            @pl.when(j // per_quarter != t)
+            def _():
+                dn_copy(j).wait_send()
+            for i in range(3):
+                out_copy(j, i).wait()
+        every(n_fs, sent_j)
+
     def in_turn(*steps):
         for name, step, *given in steps:
             with jax.named_scope(name):
@@ -764,51 +829,28 @@
     @pl.when(inner)
     def _():
         in_turn(
-            ("f0", result_of, 0), ("e2", end_hidden), ("f2", end_results),
-            ("g00", stage_g, 0, 0), ("f1", result_of, 1), ("g01", stage_g, 0, 1),
-            ("g10", stage_g, 1, 0), ("f2", result_of, 2), ("g11", stage_g, 1, 1),
-            ("f3", result_of, 3), ("g20", stage_g, 2, 0), ("g21", stage_g, 2, 1),
+            ("h", every, n_z, stage_h), ("f00", stage_f, 0, 0), ("f01", stage_f, 0, 1),
+            ("e2", end_hidden), ("z0", end_results, 0), ("z1", end_results, 1), ("g00", stage_g, 0, 0),
+            ("f10", stage_f, 1, 0), ("f11", stage_f, 1, 1), ("g01", stage_g, 0, 1), ("g10", stage_g, 1, 0),
+            ("f20", stage_f, 2, 0), ("f21", stage_f, 2, 1), ("g11", stage_g, 1, 1), ("f30", stage_f, 3, 0),
+            ("f31", stage_f, 3, 1), ("g20", stage_g, 2, 0), ("g21", stage_g, 2, 1), ("settle", settle),
             ("g30", stage_g, 3, 0), ("g31", stage_g, 3, 1),
         )
 
     @pl.when(~inner)
     def _():
         in_turn(
-            ("f1", result_of, 1), ("g10", stage_g, 1, 0), ("f2", result_of, 2), ("g11", stage_g, 1, 1),
-            ("g20", stage_g, 2, 0), ("f3", result_of, 3), ("g21", stage_g, 2, 1),
+            ("h", every, n_z, stage_h), ("f10", stage_f, 1, 0), ("f11", stage_f, 1, 1), ("g10", stage_g, 1, 0),
+            ("f20", stage_f, 2, 0), ("f21", stage_f, 2, 1), ("g11", stage_g, 1, 1), ("g20", stage_g, 2, 0),
+            ("f30", stage_f, 3, 0), ("f31", stage_f, 3, 1), ("g21", stage_g, 2, 1), ("settle", settle),
             ("g30", stage_g, 3, 0), ("g31", stage_g, 3, 1),
         )
 
-    for d in range(1, n_tp):
-        ssq_copy(d).wait_send()
-    for d in range(1, n_z):
-        aux_copy(d).wait_send()
-
-    def sent_w(d):
-        wgu_copy(d).wait_send()
-        wd_copy(d).wait_send()
-    span(1, n_fs, sent_w)
-
-    def sent_b(b):
-        @pl.when(goes_right(b) & ~(inner & (b == z - 2)))
-        def _():
-            ag_right(b).wait_send()
-
-        @pl.when(goes_left(b) & ~(inner & (b == z + 2)))
-        def _():
-            ag_left(b).wait_send()
-        for copy in (x_copy, rc_copy, ry_copy, rf_copy):
-            copy(b).wait_send()
+    def last_sent(b):
         apart = ~inner & (b == at(3))
 
-        @pl.when(apart)
-        def _():
-            h2_copy(b).wait_send()
-
         @pl.when(~apart)
         def _():
-            for copy in (hc_copy, hy_copy, hf_copy):
-                copy(b).wait_send()
             for q in range(per_quarter):
                 y_copy(b, q).wait_send()
 
@@ -821,36 +863,45 @@
         def _():
             for q in range(per_quarter):
                 rs_left(b, q).wait_send()
-    every(n_z, sent_b)
-
-    @pl.when(inner)
-    def _():
-        h2y_copy().wait_send()
-        h2c_copy().wait_send()
-        h2f_copy().wait_send()
-        for q in range(per_quarter):
+    every(n_z, last_sent)
+    for q in range(per_quarter):
+        mixed_copy(q).wait()
+
+        @pl.when(inner)
+        def _():
             y2_copy(q).wait_send()
 
-    @pl.when(~inner)
-    def _():
-        for k in range(PAIR):
-            help_copy(k).wait_send()
-
-    def sent_j(j):
-        @pl.when(inner & (j != me) & (j // PAIR != at(-1)))
-        def _():
-            wf_copy(j).wait_send()
-
-        @pl.when(inner & (j // per_quarter != t))
-        def _():
-            d2_copy(j).wait_send()
-
-        @pl.when(j // per_quarter != t)
-        def _():
-            dn_copy(j).wait_send()
-        for copy in out_copies(j):
-            copy.wait()
-    every(n_fs, sent_j)
+
+def publish_kernel(count, *refs):
+    sources, targets = refs[:count], refs[count : 2 * count]
+    buffers, (come, go) = refs[2 * count : 3 * count], refs[3 * count :]
+
+    def inward(i):
+        return pltpu.make_async_copy(sources[i], buffers[i], come.at[i])
+
+    def outward(i):
+        return pltpu.make_async_copy(buffers[i], targets[i], go.at[i])
+    for i in range(count):
+        inward(i).start()
+    for i in range(count):
+        inward(i).wait()
+        outward(i).start()
+    for i in range(count):
+        outward(i).wait()
+
+
+def publish(*arrays):
+    anywhere = pl.BlockSpec(memory_space=pl.ANY)
+    count = len(arrays)
+    return pl.pallas_call(
+        functools.partial(publish_kernel, count),
+        out_shape=tuple(jax.ShapeDtypeStruct(a.shape, a.dtype) for a in arrays),
+        in_specs=[anywhere] * count,
+        out_specs=(anywhere,) * count,
+        scratch_shapes=[pltpu.VMEM(a.shape, a.dtype) for a in arrays]
+        + [pltpu.SemaphoreType.DMA((count,))] * 2,
+        name="publish",
+    )(*arrays)
 
 
 def scratch_for(dims):
@@ -887,11 +938,11 @@
     sems = [
         (3, n_fs), (n_tp,), (n_tp,), (n_z,), (n_z,), (n_z,), (n_z,), (n_z,),
         (n_fs,), (n_fs,), (n_fs,), (n_fs,), (n_z,), (n_z,),
-        (n_z,), (n_z,), (n_z,), (n_z,), (n_z,), (n_z,),
+        (n_z,), (n_z,), (n_z, 2), (n_z, 2), (n_z,), (n_z,),
         (n_z,), (n_z,), (n_z,), (n_z,), (n_z,), (n_z,),
         (n_fs,), (per_quarter, n_tp), (n_z, per_quarter), (n_z, per_quarter),
         (n_z, per_quarter), (n_z, per_quarter), (n_z + 1, per_quarter), (3, n_fs),
-        (PAIR,), (n_fs,), (n_fs,), (n_fs,), (per_quarter, n_tp), (8,), (per_quarter,), (per_quarter,),
+        (PAIR,), (n_fs,), (n_fs,), (n_fs,), (per_quarter, n_tp), (8,), (per_quarter,), (per_quarter,), (per_quarter,),
     ]
     return buffers, sems
 
@@ -931,7 +982,7 @@
         functools.partial(moe_kernel, dims),
         out_shape=(matrix, matrix, matrix, jax.ShapeDtypeStruct((r_rows, feat), jnp.bfloat16)),
         in_specs=[vmem] * 4 + [anywhere] * 3,
-        out_specs=(anywhere, anywhere, anywhere, vmem),
+        out_specs=(anywhere, anywhere, anywhere, anywhere),
         scratch_shapes=[pltpu.VMEM(shape, kind) for shape, kind in buffers]
         + [pltpu.SemaphoreType.DMA(shape) for shape in sems],
         compiler_params=pltpu.CompilerParams(
@@ -939,6 +990,7 @@
         ),
         name="experts",
     )(tokens, norm_gain[None, :], routes.T, route_weight.T, gate_master, up_master, down_master)
+    gate_out, up_out, down_out, mixed = publish(gate_out, up_out, down_out, mixed)
     return (gate_out[None], up_out[None], down_out[None], mixed)
 
 

time: 185 us -> 182 us (0.984)
  local copies, waits for them, and re-layouts: 5.24 us -> 0 us
  Pallas kernels: 179 us -> 181 us
    unnamed x10 -> x0, local copies, waits for them, and re-layouts: 5.24 us -> none
    pallas_call x0 -> x1, Pallas kernels: none -> 3.21 us  [publish(): pl.pallas_call(functools.partial(publish_kernel, count), out_shape=tuple(...]
where the time goes in v4:
time: 182 us
  Pallas kernels  181 us (99%)
    pallas_call x1, Pallas kernels, body(): pl.pallas_call(functools.partial(moe_kernel, dims), out_shape=(matrix, ma...  178 us

profile of v4, /device:TPU:5, one launch (start us, length us, event | category | flops | bytes accessed | tf_op | source)
XLA Modules:
  0.0 182.3 jit_solution(1553561033496562673)
XLA Ops:
  0.6 178.3 %experts.1 = (bf16[4096,128]{1,0:T(8,128)(2,1)}, bf16[4096,128]{1,0:T(8,128)(2,1)}, bf16[4096,128]{1,0:T(8,128)(2,1)}, bf16[384,1024]{1,0:T(8,128)(2,1)}) custom-call(bf16[384,1024]{1,0:T(8,128)(2,1)} %tok.1, f32[1,512]{1,0:T(1,128)} %bitcast.8, s32[2,384]{1,0:T(2,128)} %bitcast.6, f32[2,384]{1,0:T(2,128)} %bitcast.7, f32[8,512,128]{2,1,0:T(8,128)} %gate_hbm.1, ...), custom_call_target="tpu_custom_call" | custom-call | tf_op jit(solution)/shard_map/experts/pallas_call | solution.py:981
  178.9 3.2 %publish.1 = (bf16[4096,128]{1,0:T(8,128)(2,1)}, bf16[4096,128]{1,0:T(8,128)(2,1)}, bf16[4096,128]{1,0:T(8,128)(2,1)}, bf16[384,1024]{1,0:T(8,128)(2,1)}) custom-call(bf16[4096,128]{1,0:T(8,128)(2,1)} %get-tuple-element.12.refs_0_, bf16[4096,128]{1,0:T(8,128)(2,1)} %get-tuple-element.13.refs_1_, bf16[4096,128]{1,0:T(8,128)(2,1)} %get-tuple-element.14.refs_2_, ...), custom_call_target="tpu_custom_call" | custom-call | tf_op jit(solution)/shard_map/publish/pallas_call | solution.py:896
